TPU v7x, 1024 devices: a whole 4x8x16 slice. The times are simulated.
1024 devices in a mesh: rep: 2 (over z_hi), fs: 64 (over z_lo, y), tp: 8 (over x, core).
Axes of the slice: x: 4, y: 8, z: 16 (z_hi: 2, z_lo: 8; z = z_hi * 8 + z_lo), core: 2. Of those that a mesh axis runs over, the one named last changes fastest.
Arguments:
- tokens: bfloat16 [65536, 2048], P(('rep', 'fs', 'tp')), may hold values from -6 to 6
- norm_gain: float32 [2048], replicated, may hold values from 0.1 to 1.9
- w_gate: bfloat16 [2048, 3072], P('fs', 'tp'), may hold values from -0.125 to 0.125
- w_up: bfloat16 [2048, 3072], P('fs', 'tp'), may hold values from -0.125 to 0.125
- w_down: bfloat16 [3072, 2048], P('tp', 'fs'), may hold values from -0.109375 to 0.109375
- post_gain: float32 [2048], replicated, may hold values from 0.1 to 1.9
Outputs:
- result: bfloat16 [65536, 2048], P(('rep', 'fs', 'tp'))
All inputs are finite; a program needn't handle non-finite values.
Results may differ from a plain program's by a relative error of at most 0.014.
Values may be sent and summed in bfloat16 or wider, within the bound.
No kernel may reach another device: no remote copies, remote signals or barrier semaphores. Data moves between devices by JAX's collectives and lax.ppermute only.
A program may use at most 32 MiB of HBM per device.

v0:
```python
import jax
import jax.numpy as jnp
from jax import lax
from jax.experimental import pallas as pl
from jax.experimental.pallas import tpu as pltpu
from jax.sharding import Mesh
from jax.sharding import PartitionSpec as P


EPS = 1e-06
ALL = ("zh", "zl", "y", "x", "c")
PLANE = ("zh", "zl", "y", "c")


def rms_scale(values, gain):
    return values * lax.rsqrt(jnp.mean(values * values, axis=-1, keepdims=True) + EPS) * gain


def copy_for_each(x, axis, length, groups=None):
    copies = jnp.broadcast_to(x[None], (length, *x.shape))
    return lax.all_to_all(copies, axis, 0, 0, tiled=True, axis_index_groups=groups)


def first_groups():
    at = lambda zh, zl, y, c: ((zh * 8 + zl) * 8 + y) * 2 + c
    groups = [[at(zh, zl, y, 0) for y in range(8)] for zh in range(2) for zl in range(8)]
    return groups + [[at(zh, zl, y, 1) for zl in range(8)] for zh in range(2) for y in range(8)]


def partner(i, kind):
    return ((i + kind) ^ 1) - kind


def exchange(x, kind):
    pairs = []
    for z in range(16):
        for y in range(8):
            here = (z * 8 + y) * 2
            pairs.append((here, (partner(z, kind) % 16 * 8 + y) * 2))
            pairs.append((here + 1, (z * 8 + partner(y, kind) % 8) * 2 + 1))
    return lax.ppermute(x, PLANE, pairs)


def ff_kernel(ids, normed, *refs):
    blocks = refs[0:8]
    keep, send, gate_w, up_w, down_w, hid = refs[8:14]
    base, core = ids[0], ids[1]
    side = 1 - 2 * (base & 1)
    weights = (gate_w, up_w, down_w)
    classes = [(base + 8 + n * side) & 7 for n in (0, 1, -1, 2, -2, 3, -3, 4)]

    @pl.when(core == 0)
    def _():
        for blk, at in zip(blocks, classes):
            for n in range(3):
                weights[n][at] = blk[:, 32 * n : 32 * n + 32, :]

    @pl.when(core == 1)
    def _():
        for blk, at in zip(blocks, classes):
            for n in range(3):
                weights[n][:, at] = blk[:, 32 * n : 32 * n + 32, :]

    x = normed[...].reshape(512, 2048)
    gate = jnp.dot(x, gate_w[...].reshape(2048, 384), preferred_element_type=jnp.float32)
    up = jnp.dot(x, up_w[...].reshape(2048, 384), preferred_element_type=jnp.float32)
    hidden = gate / (1.0 + jnp.exp(-gate)) * up
    hid[...] = hidden.astype(jnp.bfloat16).reshape(4, 2, 64, 384)
    down = down_w[...].reshape(2048, 384)
    nt = (((1,), (1,)), ((), ()))
    for out, which in ((send, 1 - core), (keep, core)):
        rows = hid[:, which].reshape(256, 384)
        part = lax.dot_general(rows, down, nt, preferred_element_type=jnp.float32)
        out[...] = part.astype(jnp.bfloat16).reshape(4, 64, 2048)


def body(tokens, norm_gain, w_gate, w_up, w_down, post_gain):
    own = jnp.concatenate([w_gate, w_up, w_down.T], axis=0)
    block = copy_for_each(own, PLANE, 8, first_groups())
    own_normed = rms_scale(tokens.astype(jnp.float32), norm_gain).astype(jnp.bfloat16)
    copies = jnp.broadcast_to(own_normed[None], (8, *own_normed.shape))
    block, copies = lax.optimization_barrier((block, copies))
    blocks = [block]
    even = odd = block
    for k in range(4):
        new_even = exchange(odd, 0)
        blocks.append(new_even)
        if k < 3:
            odd = exchange(even, 1)
            blocks.append(odd)
        even = new_even
    normed = lax.all_to_all(copies, ("x", "c"), 0, 0, tiled=True)
    core = lax.axis_index("c")
    base = jnp.where(core == 0, lax.axis_index("zl"), lax.axis_index("y"))
    ids = jnp.stack([base, core]).astype(jnp.int32)
    vmem = pl.BlockSpec(memory_space=pltpu.VMEM)
    part = jax.ShapeDtypeStruct((4, 64, 2048), jnp.bfloat16)
    whole = pltpu.VMEM((8, 8, 32, 384), jnp.bfloat16)
    keep, send = pl.pallas_call(
        ff_kernel,
        out_shape=(part, part),
        in_specs=[pl.BlockSpec(memory_space=pltpu.SMEM)] + [vmem] * 9,
        out_specs=(vmem, vmem),
        scratch_shapes=[whole, whole, whole, pltpu.VMEM((4, 2, 64, 384), jnp.bfloat16)],
        compiler_params=pltpu.CompilerParams(vmem_limit_bytes=48 * 1024 * 1024),
        name="ff",
    )(ids, normed, *blocks)
    other = lax.ppermute(send, "c", [(0, 1), (1, 0)])
    pair = (keep.astype(jnp.float32) + other.astype(jnp.float32)).astype(jnp.bfloat16)
    arrived = lax.all_to_all(pair, "x", split_axis=0, concat_axis=0, tiled=True)
    summed = arrived.astype(jnp.float32).sum(axis=0)
    return rms_scale(summed, post_gain).astype(jnp.bfloat16)


def solution(mesh):
    finer = Mesh(mesh.devices.reshape(2, 8, 8, 4, 2), ALL)
    split = P(("zl", "y"), ("x", "c"))
    return jax.shard_map(
        body,
        mesh=finer,
        in_specs=(P(ALL, None), P(), split, split, P(("x", "c"), ("zl", "y")), P()),
        out_specs=P(ALL, None),
        check_vma=False,
    )
```

profile of v0, /device:TPU:1, one launch (start us, length us, event | category | flops | bytes accessed | tf_op | source)
XLA Modules:
  0.0 123.9 jit_solution(7854658008263021544)
XLA Ops:
  0.0 0.0 copy-start
  0.0 0.0 copy-start.1
  0.0 0.8 pad_maximum_fusion
  0.8 0.9 broadcast_in_dim.4
  1.7 16.2 %all-to-all-start = ((bf16[8,96,384]{2,1,0:T(8,128)(2,1)}), bf16[8,96,384]{2,1,0:T(8,128)(2,1)S(1)}, u32[]{:S(2)}, u32[]{:S(2)}) async-start(bf16[8,96,384]{2,1,0:T(8,128)(2,1)} %broadcast_in_dim.4), calls=%async_computation | async-start | bytes 1179648 | tf_op jit(solution)/shard_map/all_to_all | solution.py:21
  17.9 0.0 copy-done
  17.9 0.2 fusion
  18.1 0.0 copy-done.1
  18.1 0.1 fusion.2
  18.2 16.1 %all-to-all-done.refs_0_ = bf16[8,96,384]{2,1,0:T(8,128)(2,1)S(1)} async-done(((bf16[8,96,384]{2,1,0:T(8,128)(2,1)}), bf16[8,96,384]{2,1,0:T(8,128)(2,1)S(1)}, u32[]{:S(2)}, u32[]{:S(2)}) %all-to-all-start) | async-done | bytes 589856 | tf_op jit(solution)/shard_map/all_to_all | solution.py:21
  34.3 1.6 %broadcast_in_dim.5 = bf16[8,64,2048]{2,1,0:T(8,128)(2,1)} broadcast(bf16[64,2048]{1,0:T(8,128)(2,1)S(1)} %fusion.2), dimensions={1,2} | broadcast | bytes 2359296 | tf_op jit(solution)/shard_map/broadcast_in_dim | solution.py:81
  35.9 8.3 %collective-permute-start.1 = (bf16[8,96,384]{2,1,0:T(8,128)(2,1)S(1)}, bf16[8,96,384]{2,1,0:T(8,128)(2,1)S(1)}, u32[]{:S(2)}, u32[]{:S(2)}) collective-permute-start(bf16[8,96,384]{2,1,0:T(8,128)(2,1)S(1)} %all-to-all-done.refs_0_), channel_id=1, source_target_pairs={{0,960},{1,57},{8,968},{9,17},{16,976},{17,9},{24,984},{25,33},{32... | collective-permute-start | bytes 1769480 | tf_op jit(solution)/shard_map/ppermute | solution.py:41
  44.2 4.4 %all-to-all-start.1 = ((bf16[8,64,2048]{2,1,0:T(8,128)(2,1)}), bf16[8,64,2048]{2,1,0:T(8,128)(2,1)}, u32[]{:S(2)}, u32[]{:S(2)}) async-start(bf16[8,64,2048]{2,1,0:T(8,128)(2,1)} %broadcast_in_dim.5), calls=%async_computation.1 | async-start | bytes 4194304 | tf_op jit(solution)/shard_map/all_to_all | solution.py:92
  48.6 1.9 %collective-permute-start = (bf16[8,96,384]{2,1,0:T(8,128)(2,1)S(1)}, bf16[8,96,384]{2,1,0:T(8,128)(2,1)S(1)}, u32[]{:S(2)}, u32[]{:S(2)}) collective-permute-start(bf16[8,96,384]{2,1,0:T(8,128)(2,1)S(1)} %all-to-all-done.refs_0_), channel_id=1, source_target_pairs={{0,64},{1,9},{8,72},{9,1},{16,80},{17,25},{24,88},{25,17},{32,96},... | collective-permute-start | bytes 1769480 | tf_op jit(solution)/shard_map/ppermute | solution.py:41
  50.6 1.0 collective-permute-done.1.refs_2_
  51.5 2.4 %collective-permute-start.2 = (bf16[8,96,384]{2,1,0:T(8,128)(2,1)S(1)}, bf16[8,96,384]{2,1,0:T(8,128)(2,1)S(1)}, u32[]{:S(2)}, u32[]{:S(2)}) collective-permute-start(bf16[8,96,384]{2,1,0:T(8,128)(2,1)S(1)} %collective-permute-done.1.refs_2_), channel_id=1, source_target_pairs={{0,64},{1,9},{8,72},{9,1},{16,80},{17,25},{24,88},{25,17},{32,96},... | collective-permute-start | bytes 1769480 | tf_op jit(solution)/shard_map/ppermute | solution.py:41
  53.9 5.7 %collective-permute-done.refs_1_ = bf16[8,96,384]{2,1,0:T(8,128)(2,1)S(1)} collective-permute-done((bf16[8,96,384]{2,1,0:T(8,128)(2,1)S(1)}, bf16[8,96,384]{2,1,0:T(8,128)(2,1)S(1)}, u32[]{:S(2)}, u32[]{:S(2)}) %collective-permute-start) | collective-permute-done | bytes 589856 | tf_op jit(solution)/shard_map/ppermute | solution.py:41
  59.6 2.5 %collective-permute-start.3 = (bf16[8,96,384]{2,1,0:T(8,128)(2,1)S(1)}, bf16[8,96,384]{2,1,0:T(8,128)(2,1)S(1)}, u32[]{:S(2)}, u32[]{:S(2)}) collective-permute-start(bf16[8,96,384]{2,1,0:T(8,128)(2,1)S(1)} %collective-permute-done.refs_1_), channel_id=1, source_target_pairs={{0,960},{1,57},{8,968},{9,17},{16,976},{17,9},{24,984},{25,33},{32... | collective-permute-start | bytes 1769480 | tf_op jit(solution)/shard_map/ppermute | solution.py:41
  62.1 3.8 %collective-permute-done.2.refs_3_ = bf16[8,96,384]{2,1,0:T(8,128)(2,1)S(1)} collective-permute-done((bf16[8,96,384]{2,1,0:T(8,128)(2,1)S(1)}, bf16[8,96,384]{2,1,0:T(8,128)(2,1)S(1)}, u32[]{:S(2)}, u32[]{:S(2)}) %collective-permute-start.2) | collective-permute-done | bytes 589856 | tf_op jit(solution)/shard_map/ppermute | solution.py:41
  65.9 2.5 %collective-permute-start.5 = (bf16[8,96,384]{2,1,0:T(8,128)(2,1)S(1)}, bf16[8,96,384]{2,1,0:T(8,128)(2,1)S(1)}, u32[]{:S(2)}, u32[]{:S(2)}) collective-permute-start(bf16[8,96,384]{2,1,0:T(8,128)(2,1)S(1)} %collective-permute-done.2.refs_3_), channel_id=1, source_target_pairs={{0,960},{1,57},{8,968},{9,17},{16,976},{17,9},{24,984},{25,33},{32... | collective-permute-start | bytes 1769480 | tf_op jit(solution)/shard_map/ppermute | solution.py:41
  68.4 3.4 %collective-permute-done.3.refs_4_ = bf16[8,96,384]{2,1,0:T(8,128)(2,1)S(1)} collective-permute-done((bf16[8,96,384]{2,1,0:T(8,128)(2,1)S(1)}, bf16[8,96,384]{2,1,0:T(8,128)(2,1)S(1)}, u32[]{:S(2)}, u32[]{:S(2)}) %collective-permute-start.3) | collective-permute-done | bytes 589856 | tf_op jit(solution)/shard_map/ppermute | solution.py:41
  71.9 1.9 %collective-permute-start.4 = (bf16[8,96,384]{2,1,0:T(8,128)(2,1)S(1)}, bf16[8,96,384]{2,1,0:T(8,128)(2,1)}, u32[]{:S(2)}, u32[]{:S(2)}) collective-permute-start(bf16[8,96,384]{2,1,0:T(8,128)(2,1)S(1)} %collective-permute-done.3.refs_4_), channel_id=1, source_target_pairs={{0,64},{1,9},{8,72},{9,1},{16,80},{17,25},{24,88},{25,17},{32,96},... | collective-permute-start | bytes 1769480 | tf_op jit(solution)/shard_map/ppermute | solution.py:41
  73.8 4.3 %collective-permute-done.5.refs_6_ = bf16[8,96,384]{2,1,0:T(8,128)(2,1)S(1)} collective-permute-done((bf16[8,96,384]{2,1,0:T(8,128)(2,1)S(1)}, bf16[8,96,384]{2,1,0:T(8,128)(2,1)S(1)}, u32[]{:S(2)}, u32[]{:S(2)}) %collective-permute-start.5) | collective-permute-done | bytes 589856 | tf_op jit(solution)/shard_map/ppermute | solution.py:41
  78.1 1.9 %collective-permute-start.6 = (bf16[8,96,384]{2,1,0:T(8,128)(2,1)S(1)}, bf16[8,96,384]{2,1,0:T(8,128)(2,1)}, u32[]{:S(2)}, u32[]{:S(2)}) collective-permute-start(bf16[8,96,384]{2,1,0:T(8,128)(2,1)S(1)} %collective-permute-done.5.refs_6_), channel_id=1, source_target_pairs={{0,64},{1,9},{8,72},{9,1},{16,80},{17,25},{24,88},{25,17},{32,96},... | collective-permute-start | bytes 1769480 | tf_op jit(solution)/shard_map/ppermute | solution.py:41
  80.0 0.1 pad_add_fusion.ids
  80.1 2.8 %collective-permute-done.4.refs_5_ = bf16[8,96,384]{2,1,0:T(8,128)(2,1)} collective-permute-done((bf16[8,96,384]{2,1,0:T(8,128)(2,1)S(1)}, bf16[8,96,384]{2,1,0:T(8,128)(2,1)}, u32[]{:S(2)}, u32[]{:S(2)}) %collective-permute-start.4) | collective-permute-done | bytes 589856 | tf_op jit(solution)/shard_map/ppermute | solution.py:41
  82.9 0.0 all-to-all-done.1.normed
  82.9 6.3 %collective-permute-done.6.refs_7_ = bf16[8,96,384]{2,1,0:T(8,128)(2,1)} collective-permute-done((bf16[8,96,384]{2,1,0:T(8,128)(2,1)S(1)}, bf16[8,96,384]{2,1,0:T(8,128)(2,1)}, u32[]{:S(2)}, u32[]{:S(2)}) %collective-permute-start.6) | collective-permute-done | bytes 589856 | tf_op jit(solution)/shard_map/ppermute | solution.py:41
  89.2 6.7 %ff.1 = (bf16[4,64,2048]{2,1,0:T(8,128)(2,1)S(1)}, bf16[4,64,2048]{2,1,0:T(8,128)(2,1)}) custom-call(s32[2]{0:T(128)S(1)} %pad_add_fusion.ids, bf16[8,64,2048]{2,1,0:T(8,128)(2,1)} %all-to-all-done.1.normed, bf16[8,96,384]{2,1,0:T(8,128)(2,1)S(1)} %all-to-all-done.refs_0_, bf16[8,96,384]{2,1,0:T(8,128)(2,1)S(1)} %collective-permute-done.refs_1_, ...), custom_call_target="tpu_custom_call" | custom-call | tf_op jit(solution)/shard_map/ff/pallas_call | solution.py:99
  95.9 5.5 %collective-permute-start.7 = (bf16[4,64,2048]{2,1,0:T(8,128)(2,1)}, bf16[4,64,2048]{2,1,0:T(8,128)(2,1)S(1)}, u32[]{:S(2)}, u32[]{:S(2)}) collective-permute-start(bf16[4,64,2048]{2,1,0:T(8,128)(2,1)} %get-tuple-element.12), channel_id=1, source_target_pairs={{0,1},{1,0},{2,3},{3,2},{4,5},{5,4},{6,7},{7,6},{8,9},{9,8},{10,11... | collective-permute-start | bytes 3145736 | tf_op jit(solution)/shard_map/ppermute | solution.py:108
  101.4 2.5 %collective-permute-done.7 = bf16[4,64,2048]{2,1,0:T(8,128)(2,1)S(1)} collective-permute-done((bf16[4,64,2048]{2,1,0:T(8,128)(2,1)}, bf16[4,64,2048]{2,1,0:T(8,128)(2,1)S(1)}, u32[]{:S(2)}, u32[]{:S(2)}) %collective-permute-start.7) | collective-permute-done | bytes 1048608 | tf_op jit(solution)/shard_map/ppermute | solution.py:108
  103.8 0.4 add_convert_fusion
  104.2 0.0 copy-start.2
  104.3 18.6 %all_to_all.15 = bf16[4,64,2048]{2,1,0:T(8,128)(2,1)S(1)} all-to-all(bf16[4,64,2048]{2,1,0:T(8,128)(2,1)S(1)} %add_convert_fusion), channel_id=1, replica_groups=mesh['zh'=2,'zl'=8,'y'=8,'x'=4,'c'=2] {'x'}, dimensions={0} | all-to-all | bytes 2097152 | tf_op jit(solution)/shard_map/all_to_all | solution.py:110
  122.8 0.2 convert_reduce_fusion
  123.0 0.1 multiply_reduce_fusion
  123.1 0.0 copy-done.2
  123.1 0.8 multiply_convert_fusion
  (2 shorter events, 0.0 us)
Async XLA Ops:
  0.0 17.9 %copy-start = (bf16[64,2048]{1,0:T(8,128)(2,1)S(1)}, bf16[64,2048]{1,0:T(8,128)(2,1)}, u32[]{:S(2)}) copy-start(bf16[64,2048]{1,0:T(8,128)(2,1)} %param.6) | copy-start | bytes 786436
  0.0 18.1 %copy-start.1 = (f32[2048]{0:T(1024)S(1)}, f32[2048]{0:T(1024)}, u32[]{:S(2)}) copy-start(f32[2048]{0:T(1024)} %param.7) | copy-start | bytes 24580
  1.7 32.7 %all-to-all-start = ((bf16[8,96,384]{2,1,0:T(8,128)(2,1)}), bf16[8,96,384]{2,1,0:T(8,128)(2,1)S(1)}, u32[]{:S(2)}, u32[]{:S(2)}) async-start(bf16[8,96,384]{2,1,0:T(8,128)(2,1)} %broadcast_in_dim.4), calls=%async_computation | async-start | bytes 1179648 | tf_op jit(solution)/shard_map/all_to_all | solution.py:21
  35.9 15.6 %collective-permute-start.1 = (bf16[8,96,384]{2,1,0:T(8,128)(2,1)S(1)}, bf16[8,96,384]{2,1,0:T(8,128)(2,1)S(1)}, u32[]{:S(2)}, u32[]{:S(2)}) collective-permute-start(bf16[8,96,384]{2,1,0:T(8,128)(2,1)S(1)} %all-to-all-done.refs_0_), channel_id=1, source_target_pairs={{0,960},{1,57},{8,968},{9,17},{16,976},{17,9},{24,984},{25,33},{32... | collective-permute-start | bytes 1769480 | tf_op jit(solution)/shard_map/ppermute | solution.py:41
  44.2 38.7 %all-to-all-start.1 = ((bf16[8,64,2048]{2,1,0:T(8,128)(2,1)}), bf16[8,64,2048]{2,1,0:T(8,128)(2,1)}, u32[]{:S(2)}, u32[]{:S(2)}) async-start(bf16[8,64,2048]{2,1,0:T(8,128)(2,1)} %broadcast_in_dim.5), calls=%async_computation.1 | async-start | bytes 4194304 | tf_op jit(solution)/shard_map/all_to_all | solution.py:92
  48.6 11.0 %collective-permute-start = (bf16[8,96,384]{2,1,0:T(8,128)(2,1)S(1)}, bf16[8,96,384]{2,1,0:T(8,128)(2,1)S(1)}, u32[]{:S(2)}, u32[]{:S(2)}) collective-permute-start(bf16[8,96,384]{2,1,0:T(8,128)(2,1)S(1)} %all-to-all-done.refs_0_), channel_id=1, source_target_pairs={{0,64},{1,9},{8,72},{9,1},{16,80},{17,25},{24,88},{25,17},{32,96},... | collective-permute-start | bytes 1769480 | tf_op jit(solution)/shard_map/ppermute | solution.py:41
  51.5 14.4 %collective-permute-start.2 = (bf16[8,96,384]{2,1,0:T(8,128)(2,1)S(1)}, bf16[8,96,384]{2,1,0:T(8,128)(2,1)S(1)}, u32[]{:S(2)}, u32[]{:S(2)}) collective-permute-start(bf16[8,96,384]{2,1,0:T(8,128)(2,1)S(1)} %collective-permute-done.1.refs_2_), channel_id=1, source_target_pairs={{0,64},{1,9},{8,72},{9,1},{16,80},{17,25},{24,88},{25,17},{32,96},... | collective-permute-start | bytes 1769480 | tf_op jit(solution)/shard_map/ppermute | solution.py:41
  59.6 12.2 %collective-permute-start.3 = (bf16[8,96,384]{2,1,0:T(8,128)(2,1)S(1)}, bf16[8,96,384]{2,1,0:T(8,128)(2,1)S(1)}, u32[]{:S(2)}, u32[]{:S(2)}) collective-permute-start(bf16[8,96,384]{2,1,0:T(8,128)(2,1)S(1)} %collective-permute-done.refs_1_), channel_id=1, source_target_pairs={{0,960},{1,57},{8,968},{9,17},{16,976},{17,9},{24,984},{25,33},{32... | collective-permute-start | bytes 1769480 | tf_op jit(solution)/shard_map/ppermute | solution.py:41
  65.9 12.1 %collective-permute-start.5 = (bf16[8,96,384]{2,1,0:T(8,128)(2,1)S(1)}, bf16[8,96,384]{2,1,0:T(8,128)(2,1)S(1)}, u32[]{:S(2)}, u32[]{:S(2)}) collective-permute-start(bf16[8,96,384]{2,1,0:T(8,128)(2,1)S(1)} %collective-permute-done.2.refs_3_), channel_id=1, source_target_pairs={{0,960},{1,57},{8,968},{9,17},{16,976},{17,9},{24,984},{25,33},{32... | collective-permute-start | bytes 1769480 | tf_op jit(solution)/shard_map/ppermute | solution.py:41
  71.9 11.0 %collective-permute-start.4 = (bf16[8,96,384]{2,1,0:T(8,128)(2,1)S(1)}, bf16[8,96,384]{2,1,0:T(8,128)(2,1)}, u32[]{:S(2)}, u32[]{:S(2)}) collective-permute-start(bf16[8,96,384]{2,1,0:T(8,128)(2,1)S(1)} %collective-permute-done.3.refs_4_), channel_id=1, source_target_pairs={{0,64},{1,9},{8,72},{9,1},{16,80},{17,25},{24,88},{25,17},{32,96},... | collective-permute-start | bytes 1769480 | tf_op jit(solution)/shard_map/ppermute | solution.py:41
  78.1 11.1 %collective-permute-start.6 = (bf16[8,96,384]{2,1,0:T(8,128)(2,1)S(1)}, bf16[8,96,384]{2,1,0:T(8,128)(2,1)}, u32[]{:S(2)}, u32[]{:S(2)}) collective-permute-start(bf16[8,96,384]{2,1,0:T(8,128)(2,1)S(1)} %collective-permute-done.5.refs_6_), channel_id=1, source_target_pairs={{0,64},{1,9},{8,72},{9,1},{16,80},{17,25},{24,88},{25,17},{32,96},... | collective-permute-start | bytes 1769480 | tf_op jit(solution)/shard_map/ppermute | solution.py:41
  95.9 8.0 %collective-permute-start.7 = (bf16[4,64,2048]{2,1,0:T(8,128)(2,1)}, bf16[4,64,2048]{2,1,0:T(8,128)(2,1)S(1)}, u32[]{:S(2)}, u32[]{:S(2)}) collective-permute-start(bf16[4,64,2048]{2,1,0:T(8,128)(2,1)} %get-tuple-element.12), channel_id=1, source_target_pairs={{0,1},{1,0},{2,3},{3,2},{4,5},{5,4},{6,7},{7,6},{8,9},{9,8},{10,11... | collective-permute-start | bytes 3145736 | tf_op jit(solution)/shard_map/ppermute | solution.py:108
  104.2 18.9 %copy-start.2 = (f32[2048]{0:T(1024)S(1)}, f32[2048]{0:T(1024)}, u32[]{:S(2)}) copy-start(f32[2048]{0:T(1024)} %param.11) | copy-start | bytes 24580
where the time goes:
time: 125 us; the launch traced here: 124 us
  starting transfers between devices  47.5 us (38%)
  waiting for transfers between devices  45.9 us (37%)
  blocking collectives  18.6 us (15%)
  Pallas kernels  6.67 us (5%)
  other arithmetic  2.7 us (2%)
  local copies, waits for them, and re-layouts  2.44 us (2%)
    ppermute x7, waiting for transfers between devices, exchange(): return lax.ppermute(x, PLANE, pairs)  27.3 us
    ppermute x7, starting transfers between devices, exchange(): return lax.ppermute(x, PLANE, pairs)  21.4 us
    all_to_all x1, blocking collectives, body(): arrived = lax.all_to_all(pair, 'x', split_axis=0, concat_axis=0, tiled=True)  18.6 us
    all_to_all x1, starting transfers between devices, copy_for_each(): lax.all_to_all(copies, axis, 0, 0, tiled=True, axis_index_groups=groups)  16.2 us
    all_to_all x1, waiting for transfers between devices, copy_for_each(): lax.all_to_all(copies, axis, 0, 0, tiled=True, axis_index_groups=groups)  16.1 us
    pallas_call x1, Pallas kernels, body(): pl.pallas_call(ff_kernel, out_shape=(part, part), in_specs=[pl.BlockSpec(...  6.67 us
    ppermute x1, starting transfers between devices, body(): other = lax.ppermute(send, 'c', [(0, 1), (1, 0)])  5.5 us
    all_to_all x1, starting transfers between devices, body(): normed = lax.all_to_all(copies, ('x', 'c'), 0, 0, tiled=True)  4.42 us
  transfers between devices with their start and end apart: 10, of which 9 were waited for; matrix products, arithmetic and copies ran while one was open for 0% of the time, Pallas kernels for 0%

commit v1 on v0

v1 whole, which is shorter than its diff:
```python
import jax
import jax.numpy as jnp
from jax import lax
from jax.experimental import pallas as pl
from jax.experimental.pallas import tpu as pltpu
from jax.sharding import Mesh
from jax.sharding import PartitionSpec as P


EPS = 1e-06
ALL = ("zh", "zl", "y", "x", "c")
PLANE = ("zh", "zl", "y", "c")


def rms_scale(values, gain):
    return values * lax.rsqrt(jnp.mean(values * values, axis=-1, keepdims=True) + EPS) * gain


def first_groups():
    at = lambda zh, zl, y, c: ((zh * 8 + zl) * 8 + y) * 2 + c
    groups = [[at(zh, zl, y, 0) for y in range(8)] for zh in range(2) for zl in range(8)]
    return groups + [[at(zh, zl, y, 1) for zl in range(8)] for zh in range(2) for y in range(8)]


def partner(i, kind):
    return ((i + kind) ^ 1) - kind


def exchange(x, kind):
    pairs = []
    for z in range(16):
        for y in range(8):
            here = (z * 8 + y) * 2
            pairs.append((here, (partner(z, kind) % 16 * 8 + y) * 2))
            pairs.append((here + 1, (z * 8 + partner(y, kind) % 8) * 2 + 1))
    return lax.ppermute(x, PLANE, pairs)


def most_kernel(ids, normed, *refs):
    blocks = refs[0:7]
    gate_up, x_last, down, gate_w, up_w = refs[7:12]
    base, core = ids[0], ids[1]
    side = 1 - 2 * (base & 1)
    weights = (gate_w, up_w, down)
    classes = [(base + 8 + n * side) & 7 for n in (0, 1, -1, 2, -2, 3, -3)]
    last = (base + 4) & 7
    empty = jnp.zeros((8, 32, 384), jnp.bfloat16)

    @pl.when(core == 0)
    def _():
        for n, w in enumerate(weights):
            w[last] = empty
            for blk, at in zip(blocks, classes):
                w[at] = blk[:, 32 * n : 32 * n + 32, :]

    @pl.when(core == 1)
    def _():
        for n, w in enumerate(weights):
            w[:, last] = empty
            for blk, at in zip(blocks, classes):
                w[:, at] = blk[:, 32 * n : 32 * n + 32, :]

    x = normed[...].reshape(512, 2048)
    for n, w in enumerate((gate_w, up_w)):
        acc = jnp.dot(x, w[...].reshape(2048, 384), preferred_element_type=jnp.float32)
        gate_up[n] = acc.reshape(4, 2, 64, 384)
    row = lax.broadcasted_iota(jnp.int32, (2048, 256), 0)
    j = lax.broadcasted_iota(jnp.int32, (2048, 256), 1)
    wanted = jnp.where(core == 0, last * 256 + j, (j >> 5) * 256 + last * 32 + (j & 31))
    pick = jnp.where(row == wanted, 1.0, 0.0).astype(jnp.bfloat16)
    picked = jnp.dot(x, pick, preferred_element_type=jnp.float32)
    x_last[...] = picked.astype(jnp.bfloat16).reshape(4, 2, 64, 256)


def last_kernel(ids, gate_up, x_last, most_down, half_0, half_1, out, down):
    base, core, which = ids[0], ids[1], ids[2]
    last = (base + 4) & 7
    halves = (half_0, half_1)
    down[...] = most_down[...]

    @pl.when(core == 0)
    def _():
        for h, half in enumerate(halves):
            down[last, 4 * h : 4 * h + 4] = half[:, 64:96, :]

    @pl.when(core == 1)
    def _():
        for h, half in enumerate(halves):
            down[4 * h : 4 * h + 4, last] = half[:, 64:96, :]

    x = x_last[:, which].reshape(256, 256)
    sums = []
    for n in range(2):
        acc = gate_up[n, :, which].reshape(256, 384)
        for h, half in enumerate(halves):
            w = half[:, 32 * n : 32 * n + 32, :].reshape(128, 384)
            acc = acc + jnp.dot(x[:, 128 * h : 128 * h + 128], w, preferred_element_type=jnp.float32)
        sums.append(acc)
    gate, up = sums
    hidden = (gate / (1.0 + jnp.exp(-gate)) * up).astype(jnp.bfloat16)
    nt = (((1,), (1,)), ((), ()))
    part = lax.dot_general(hidden, down[...].reshape(2048, 384), nt, preferred_element_type=jnp.float32)
    out[...] = part.astype(jnp.bfloat16).reshape(4, 64, 2048)


VMEM = pl.BlockSpec(memory_space=pltpu.VMEM)
SMEM = pl.BlockSpec(memory_space=pltpu.SMEM)
WHOLE = (8, 8, 32, 384)


def most_of(ids, normed, blocks):
    return pl.pallas_call(
        most_kernel,
        out_shape=(
            jax.ShapeDtypeStruct((2, 4, 2, 64, 384), jnp.float32),
            jax.ShapeDtypeStruct((4, 2, 64, 256), jnp.bfloat16),
            jax.ShapeDtypeStruct(WHOLE, jnp.bfloat16),
        ),
        in_specs=[SMEM] + [VMEM] * 8,
        out_specs=(VMEM, VMEM, VMEM),
        scratch_shapes=[pltpu.VMEM(WHOLE, jnp.bfloat16)] * 2,
        compiler_params=pltpu.CompilerParams(vmem_limit_bytes=50 * 1024 * 1024),
        name="most",
    )(ids, normed, *blocks)


def partial_of(ids, most, halves):
    return pl.pallas_call(
        last_kernel,
        out_shape=jax.ShapeDtypeStruct((4, 64, 2048), jnp.bfloat16),
        in_specs=[SMEM] + [VMEM] * 5,
        out_specs=VMEM,
        scratch_shapes=[pltpu.VMEM(WHOLE, jnp.bfloat16)],
        compiler_params=pltpu.CompilerParams(vmem_limit_bytes=16 * 1024 * 1024),
    )(ids, *most, *halves)


def body(tokens, norm_gain, w_gate, w_up, w_down, post_gain):
    own = jnp.concatenate([w_gate, w_up, w_down.T], axis=0)
    own = jnp.broadcast_to(own[None], (8, *own.shape))
    block = lax.all_to_all(own, PLANE, 0, 0, tiled=True, axis_index_groups=first_groups())
    own_normed = rms_scale(tokens.astype(jnp.float32), norm_gain).astype(jnp.bfloat16)
    copies = jnp.broadcast_to(own_normed[None], (8, *own_normed.shape))
    block, copies = lax.optimization_barrier((block, copies))
    blocks = [block]
    even = odd = block
    for _ in range(3):
        new_even = exchange(odd, 0)
        odd = exchange(even, 1)
        even = new_even
        blocks += [even, odd]
    half_0 = exchange(odd[:4], 0)
    half_1 = exchange(even[4:], 1)
    normed = lax.all_to_all(copies, ("x", "c"), 0, 0, tiled=True)
    core = lax.axis_index("c")
    base = jnp.where(core == 0, lax.axis_index("zl"), lax.axis_index("y"))
    ids = jnp.stack([base, core, 1 - core]).astype(jnp.int32)
    most = most_of(ids, normed, blocks)
    send = partial_of(ids, most, (half_0, half_1))
    other = lax.ppermute(send, "c", [(0, 1), (1, 0)])
    ids = jnp.stack([base, core, core]).astype(jnp.int32)
    keep = partial_of(ids, most, (half_0, half_1))
    pair = (keep.astype(jnp.float32) + other.astype(jnp.float32)).astype(jnp.bfloat16)
    arrived = lax.all_to_all(pair, "x", split_axis=0, concat_axis=0, tiled=True)
    summed = arrived.astype(jnp.float32).sum(axis=0)
    return rms_scale(summed, post_gain).astype(jnp.bfloat16)


def solution(mesh):
    finer = Mesh(mesh.devices.reshape(2, 8, 8, 4, 2), ALL)
    split = P(("zl", "y"), ("x", "c"))
    return jax.shard_map(
        body,
        mesh=finer,
        in_specs=(P(ALL, None), P(), split, split, P(("x", "c"), ("zl", "y")), P()),
        out_specs=P(ALL, None),
        check_vma=False,
    )
```

time: 125 us -> 124 us (level)
  waiting for transfers between devices: 45.9 us -> 29.2 us
  local copies, waits for them, and re-layouts: 2.44 us -> 8.68 us
  starting transfers between devices: 47.5 us -> 53.3 us
  Pallas kernels: 6.67 us -> 9.56 us
    ppermute x7 -> x8, waiting for transfers between devices: 27.3 us -> 12.6 us  [exchange(): return lax.ppermute(x, PLANE, pairs)]
    ppermute x7 -> x8, starting transfers between devices: 21.4 us -> 28.2 us  [exchange(): return lax.ppermute(x, PLANE, pairs)]
    unnamed x6 -> x20, local copies, waits for them, and re-layouts: 0.01 us -> 4.76 us
    pallas_call x1 -> x3, Pallas kernels: 6.67 us -> 9.56 us  [the longest x1 6.17 us: most_of(): pl.pallas_call(most_kernel, out_shape=(jax.ShapeDtypeStruct((2, 4, 2, 64,...]
    ppermute x1, waiting for transfers between devices: 2.48 us -> 0.48 us  [body(): other = lax.ppermute(send, 'c', [(0, 1), (1, 0)])]
    slice x0 -> x2, local copies, waits for them, and re-layouts: none -> 1.48 us  [the longest x1 0.74 us: body(): half_0 = exchange(odd[:4], 0)]
  transfers between devices with their start and end apart: 10 -> 11, of which waited for: 9 -> 8; matrix products, arithmetic and copies ran while one was open for 0% -> 2% of each run, Pallas kernels for 0% -> 6%
where the time goes in v1:
time: 124 us; the launch traced here: 122 us
  starting transfers between devices  53.3 us (43%)
  waiting for transfers between devices  29.2 us (24%)
  blocking collectives  18.4 us (15%)
  Pallas kernels  9.56 us (8%)
  local copies, waits for them, and re-layouts  8.68 us (7%)
  other arithmetic  2.78 us (2%)
    ppermute x8, starting transfers between devices, exchange(): return lax.ppermute(x, PLANE, pairs)  28.2 us
    all_to_all x1, blocking collectives, body(): arrived = lax.all_to_all(pair, 'x', split_axis=0, concat_axis=0, tiled=True)  18.4 us
    all_to_all x1, starting transfers between devices, body(): lax.all_to_all(own, PLANE, 0, 0, tiled=True, axis_index_groups=first_grou...  16.2 us
    all_to_all x1, waiting for transfers between devices, body(): lax.all_to_all(own, PLANE, 0, 0, tiled=True, axis_index_groups=first_grou...  16.1 us
    ppermute x8, waiting for transfers between devices, exchange(): return lax.ppermute(x, PLANE, pairs)  12.6 us
    pallas_call x1, Pallas kernels, most_of(): pl.pallas_call(most_kernel, out_shape=(jax.ShapeDtypeStruct((2, 4, 2, 64,...  6.17 us
    unnamed x20, local copies, waits for them, and re-layouts  4.76 us
    all_to_all x1, starting transfers between devices, body(): normed = lax.all_to_all(copies, ('x', 'c'), 0, 0, tiled=True)  4.42 us
  transfers between devices with their start and end apart: 11, of which 8 were waited for; matrix products, arithmetic and copies ran while one was open for 2% of the time, Pallas kernels for 6%

profile of v1, /device:TPU:1, one launch (start us, length us, event | category | flops | bytes accessed | tf_op | source)
XLA Modules:
  0.0 122.1 jit_solution(7169494875993228561)
XLA Ops:
  0.0 0.0 copy-start.7
  0.0 0.0 copy-start.8
  0.0 0.8 pad_maximum_fusion
  0.8 0.9 broadcast_in_dim.4
  1.7 16.2 %all-to-all-start = ((bf16[8,96,384]{2,1,0:T(8,128)(2,1)}), bf16[8,96,384]{2,1,0:T(8,128)(2,1)S(1)}, u32[]{:S(2)}, u32[]{:S(2)}) async-start(bf16[8,96,384]{2,1,0:T(8,128)(2,1)} %broadcast_in_dim.4), calls=%async_computation | async-start | bytes 1179648 | tf_op jit(solution)/shard_map/all_to_all | solution.py:141
  17.9 0.0 copy-done.7
  17.9 0.2 fusion
  18.1 0.0 copy-done.8
  18.1 0.1 fusion.2
  18.3 16.1 %all-to-all-done.refs_0_ = bf16[8,96,384]{2,1,0:T(8,128)(2,1)S(1)} async-done(((bf16[8,96,384]{2,1,0:T(8,128)(2,1)}), bf16[8,96,384]{2,1,0:T(8,128)(2,1)S(1)}, u32[]{:S(2)}, u32[]{:S(2)}) %all-to-all-start) | async-done | bytes 589856 | tf_op jit(solution)/shard_map/all_to_all | solution.py:141
  34.4 1.6 %broadcast_in_dim.5 = bf16[8,64,2048]{2,1,0:T(8,128)(2,1)} broadcast(bf16[64,2048]{1,0:T(8,128)(2,1)S(1)} %fusion.2), dimensions={1,2} | broadcast | bytes 2359296 | tf_op jit(solution)/shard_map/broadcast_in_dim | solution.py:143
  35.9 8.3 %collective-permute-start.1 = (bf16[8,96,384]{2,1,0:T(8,128)(2,1)S(1)}, bf16[8,96,384]{2,1,0:T(8,128)(2,1)S(1)}, u32[]{:S(2)}, u32[]{:S(2)}) collective-permute-start(bf16[8,96,384]{2,1,0:T(8,128)(2,1)S(1)} %all-to-all-done.refs_0_), channel_id=1, source_target_pairs={{0,960},{1,57},{8,968},{9,17},{16,976},{17,9},{24,984},{25,33},{32... | collective-permute-start | bytes 1769480 | tf_op jit(solution)/shard_map/ppermute | solution.py:36
  44.3 1.9 %collective-permute-start = (bf16[8,96,384]{2,1,0:T(8,128)(2,1)S(1)}, bf16[8,96,384]{2,1,0:T(8,128)(2,1)S(1)}, u32[]{:S(2)}, u32[]{:S(2)}) collective-permute-start(bf16[8,96,384]{2,1,0:T(8,128)(2,1)S(1)} %all-to-all-done.refs_0_), channel_id=1, source_target_pairs={{0,64},{1,9},{8,72},{9,1},{16,80},{17,25},{24,88},{25,17},{32,96},... | collective-permute-start | bytes 1769480 | tf_op jit(solution)/shard_map/ppermute | solution.py:36
  46.2 4.4 %all-to-all-start.1 = ((bf16[8,64,2048]{2,1,0:T(8,128)(2,1)}), bf16[8,64,2048]{2,1,0:T(8,128)(2,1)}, u32[]{:S(2)}, u32[]{:S(2)}) async-start(bf16[8,64,2048]{2,1,0:T(8,128)(2,1)} %broadcast_in_dim.5), calls=%async_computation.1 | async-start | bytes 4194304 | tf_op jit(solution)/shard_map/all_to_all | solution.py:154
  50.6 0.9 collective-permute-done.1.refs_2_
  51.5 2.4 %collective-permute-start.2 = (bf16[8,96,384]{2,1,0:T(8,128)(2,1)S(1)}, bf16[8,96,384]{2,1,0:T(8,128)(2,1)S(1)}, u32[]{:S(2)}, u32[]{:S(2)}) collective-permute-start(bf16[8,96,384]{2,1,0:T(8,128)(2,1)S(1)} %collective-permute-done.1.refs_2_), channel_id=1, source_target_pairs={{0,64},{1,9},{8,72},{9,1},{16,80},{17,25},{24,88},{25,17},{32,96},... | collective-permute-start | bytes 1769480 | tf_op jit(solution)/shard_map/ppermute | solution.py:36
  54.0 1.3 %collective-permute-done.refs_1_ = bf16[8,96,384]{2,1,0:T(8,128)(2,1)S(1)} collective-permute-done((bf16[8,96,384]{2,1,0:T(8,128)(2,1)S(1)}, bf16[8,96,384]{2,1,0:T(8,128)(2,1)S(1)}, u32[]{:S(2)}, u32[]{:S(2)}) %collective-permute-start) | collective-permute-done | bytes 589856 | tf_op jit(solution)/shard_map/ppermute | solution.py:36
  55.3 2.7 %collective-permute-start.3 = (bf16[8,96,384]{2,1,0:T(8,128)(2,1)S(1)}, bf16[8,96,384]{2,1,0:T(8,128)(2,1)S(1)}, u32[]{:S(2)}, u32[]{:S(2)}) collective-permute-start(bf16[8,96,384]{2,1,0:T(8,128)(2,1)S(1)} %collective-permute-done.refs_1_), channel_id=1, source_target_pairs={{0,960},{1,57},{8,968},{9,17},{16,976},{17,9},{24,984},{25,33},{32... | collective-permute-start | bytes 1769480 | tf_op jit(solution)/shard_map/ppermute | solution.py:36
  58.0 4.5 %collective-permute-done.2.refs_3_ = bf16[8,96,384]{2,1,0:T(8,128)(2,1)S(1)} collective-permute-done((bf16[8,96,384]{2,1,0:T(8,128)(2,1)S(1)}, bf16[8,96,384]{2,1,0:T(8,128)(2,1)S(1)}, u32[]{:S(2)}, u32[]{:S(2)}) %collective-permute-start.2) | collective-permute-done | bytes 589856 | tf_op jit(solution)/shard_map/ppermute | solution.py:36
  62.5 4.6 %collective-permute-start.5 = (bf16[8,96,384]{2,1,0:T(8,128)(2,1)S(1)}, bf16[8,96,384]{2,1,0:T(8,128)(2,1)S(1)}, u32[]{:S(2)}, u32[]{:S(2)}) collective-permute-start(bf16[8,96,384]{2,1,0:T(8,128)(2,1)S(1)} %collective-permute-done.2.refs_3_), channel_id=1, source_target_pairs={{0,960},{1,57},{8,968},{9,17},{16,976},{17,9},{24,984},{25,33},{32... | collective-permute-start | bytes 1769480 | tf_op jit(solution)/shard_map/ppermute | solution.py:36
  67.1 0.4 collective-permute-done.3.refs_4_
  67.5 0.0 copy-start.4
  67.5 1.9 %collective-permute-start.4 = (bf16[8,96,384]{2,1,0:T(8,128)(2,1)S(1)}, bf16[8,96,384]{2,1,0:T(8,128)(2,1)S(1)}, u32[]{:S(2)}, u32[]{:S(2)}) collective-permute-start(bf16[8,96,384]{2,1,0:T(8,128)(2,1)S(1)} %collective-permute-done.3.refs_4_), channel_id=1, source_target_pairs={{0,64},{1,9},{8,72},{9,1},{16,80},{17,25},{24,88},{25,17},{32,96},... | collective-permute-start | bytes 1769480 | tf_op jit(solution)/shard_map/ppermute | solution.py:36
  69.4 5.3 %collective-permute-done.5.refs_6_ = bf16[8,96,384]{2,1,0:T(8,128)(2,1)S(1)} collective-permute-done((bf16[8,96,384]{2,1,0:T(8,128)(2,1)S(1)}, bf16[8,96,384]{2,1,0:T(8,128)(2,1)S(1)}, u32[]{:S(2)}, u32[]{:S(2)}) %collective-permute-start.5) | collective-permute-done | bytes 589856 | tf_op jit(solution)/shard_map/ppermute | solution.py:36
  74.8 0.0 copy-start.6
  74.8 0.9 copy-done.6
  75.6 0.7 slice.8
  76.4 1.9 %collective-permute-start.6 = (bf16[4,96,384]{2,1,0:T(8,128)(2,1)}, bf16[4,96,384]{2,1,0:T(8,128)(2,1)S(1)}, u32[]{:S(2)}, u32[]{:S(2)}) collective-permute-start(bf16[4,96,384]{2,1,0:T(8,128)(2,1)} %slice.8), channel_id=1, source_target_pairs={{0,64},{1,9},{8,72},{9,1},{16,80},{17,25},{24,88},{25,17},{32,96},... | collective-permute-start | bytes 884744 | tf_op jit(solution)/shard_map/ppermute | solution.py:36
  78.3 0.1 collective-permute-done.4.refs_5_
  78.4 0.0 copy-done.4
  78.4 0.7 slice.9
  79.2 4.4 %collective-permute-start.7 = (bf16[4,96,384]{2,1,0:T(8,128)(2,1)}, bf16[4,96,384]{2,1,0:T(8,128)(2,1)S(1)}, u32[]{:S(2)}, u32[]{:S(2)}) collective-permute-start(bf16[4,96,384]{2,1,0:T(8,128)(2,1)} %slice.9), channel_id=1, source_target_pairs={{0,960},{1,57},{8,968},{9,17},{16,976},{17,9},{24,984},{25,33},{32... | collective-permute-start | bytes 884744 | tf_op jit(solution)/shard_map/ppermute | solution.py:36
  83.6 0.1 pad_add_fusion.2.ids
  83.7 0.0 all-to-all-done.1.normed
  83.7 0.0 copy-start.5
  83.7 1.1 copy-done.5
  84.8 6.2 %most.1 = (f32[2,4,2,64,384]{4,3,2,1,0:T(8,128)}, bf16[4,2,64,256]{3,2,1,0:T(8,128)(2,1)S(1)}, bf16[8,8,32,384]{3,2,1,0:T(8,128)(2,1)}) custom-call(s32[3]{0:T(128)S(1)} %pad_add_fusion.2.ids, bf16[8,64,2048]{2,1,0:T(8,128)(2,1)} %all-to-all-done.1.normed, bf16[8,96,384]{2,1,0:T(8,128)(2,1)S(1)} %all-to-all-done.refs_0_, ...), custom_call_target="tpu_custom_call" | custom-call | tf_op jit(solution)/shard_map/most/pallas_call | solution.py:112
  90.9 0.0 collective-permute-done.6.half_0
  90.9 0.0 collective-permute-done.7.half_1
  90.9 0.0 copy-start
  91.0 1.4 %copy-done = f32[2,4,2,64,384]{4,3,2,1,0:T(8,128)S(1)} copy-done((f32[2,4,2,64,384]{4,3,2,1,0:T(8,128)S(1)}, f32[2,4,2,64,384]{4,3,2,1,0:T(8,128)}, u32[]{:S(2)}) %copy-start) | copy-done | bytes 1572888
  92.4 0.0 copy-start.2
  92.4 1.4 %copy-done.2 = bf16[8,8,32,384]{3,2,1,0:T(8,128)(2,1)S(1)} copy-done((bf16[8,8,32,384]{3,2,1,0:T(8,128)(2,1)S(1)}, bf16[8,8,32,384]{3,2,1,0:T(8,128)(2,1)}, u32[]{:S(2)}) %copy-start.2) | copy-done | bytes 1572888
  93.8 0.0 copy-start.1
  93.8 0.0 copy-start.3
  93.8 1.7 %shard_map.65 = bf16[4,64,2048]{2,1,0:T(8,128)(2,1)S(1)} custom-call(s32[3]{0:T(128)S(1)} %pad_add_fusion.2.ids, f32[2,4,2,64,384]{4,3,2,1,0:T(8,128)S(1)} %copy-done, bf16[4,2,64,256]{3,2,1,0:T(8,128)(2,1)S(1)} %get-tuple-element.13.x_last, bf16[8,8,32,384]{3,2,1,0:T(8,128)(2,1)S(1)} %copy-done.2, bf16[4,96,384]{2,1,0:T(8,128)(2,1)S(1)} %collective-permute-done.6.half_0, ...), custom_call_target="tpu_custom_call" | custom-call | tf_op jit(solution)/shard_map/pallas_call | solution.py:128
  95.5 4.4 %collective-permute-start.8 = (bf16[4,64,2048]{2,1,0:T(8,128)(2,1)S(1)}, bf16[4,64,2048]{2,1,0:T(8,128)(2,1)S(1)}, u32[]{:S(2)}, u32[]{:S(2)}) collective-permute-start(bf16[4,64,2048]{2,1,0:T(8,128)(2,1)S(1)} %shard_map.65), channel_id=1, source_target_pairs={{0,1},{1,0},{2,3},{3,2},{4,5},{5,4},{6,7},{7,6},{8,9},{9,8},{10,11... | collective-permute-start | bytes 3145736 | tf_op jit(solution)/shard_map/ppermute | solution.py:160
  99.8 0.1 pad_add_fusion.ids
  99.9 0.0 copy-done.1
  99.9 0.0 copy-done.3
  99.9 1.7 %shard_map.64 = bf16[4,64,2048]{2,1,0:T(8,128)(2,1)S(1)} custom-call(s32[3]{0:T(128)S(1)} %pad_add_fusion.ids, f32[2,4,2,64,384]{4,3,2,1,0:T(8,128)S(1)} %copy-done.1, bf16[4,2,64,256]{3,2,1,0:T(8,128)(2,1)S(1)} %get-tuple-element.13.x_last, bf16[8,8,32,384]{3,2,1,0:T(8,128)(2,1)S(1)} %copy-done.3, bf16[4,96,384]{2,1,0:T(8,128)(2,1)S(1)} %collective-permute-done.6.half_0, ...), custom_call_target="tpu_custom_call" | custom-call | tf_op jit(solution)/shard_map/pallas_call | solution.py:128
  101.6 0.5 collective-permute-done.8
  102.1 0.4 add_convert_fusion
  102.5 0.0 copy-start.9
  102.5 18.4 %all_to_all.15 = bf16[4,64,2048]{2,1,0:T(8,128)(2,1)S(1)} all-to-all(bf16[4,64,2048]{2,1,0:T(8,128)(2,1)S(1)} %add_convert_fusion), channel_id=1, replica_groups=mesh['zh'=2,'zl'=8,'y'=8,'x'=4,'c'=2] {'x'}, dimensions={0} | all-to-all | bytes 2097152 | tf_op jit(solution)/shard_map/all_to_all | solution.py:164
  121.0 0.2 convert_reduce_fusion
  121.1 0.1 multiply_reduce_fusion
  121.3 0.0 copy-done.9
  121.3 0.8 multiply_convert_fusion
  (2 shorter events, 0.0 us)
Async XLA Ops:
  0.0 17.9 %copy-start.7 = (bf16[64,2048]{1,0:T(8,128)(2,1)S(1)}, bf16[64,2048]{1,0:T(8,128)(2,1)}, u32[]{:S(2)}) copy-start(bf16[64,2048]{1,0:T(8,128)(2,1)} %param.6) | copy-start | bytes 786436
  0.0 18.1 %copy-start.8 = (f32[2048]{0:T(1024)S(1)}, f32[2048]{0:T(1024)}, u32[]{:S(2)}) copy-start(f32[2048]{0:T(1024)} %param.7) | copy-start | bytes 24580
  1.7 32.7 %all-to-all-start = ((bf16[8,96,384]{2,1,0:T(8,128)(2,1)}), bf16[8,96,384]{2,1,0:T(8,128)(2,1)S(1)}, u32[]{:S(2)}, u32[]{:S(2)}) async-start(bf16[8,96,384]{2,1,0:T(8,128)(2,1)} %broadcast_in_dim.4), calls=%async_computation | async-start | bytes 1179648 | tf_op jit(solution)/shard_map/all_to_all | solution.py:141
  35.9 15.6 %collective-permute-start.1 = (bf16[8,96,384]{2,1,0:T(8,128)(2,1)S(1)}, bf16[8,96,384]{2,1,0:T(8,128)(2,1)S(1)}, u32[]{:S(2)}, u32[]{:S(2)}) collective-permute-start(bf16[8,96,384]{2,1,0:T(8,128)(2,1)S(1)} %all-to-all-done.refs_0_), channel_id=1, source_target_pairs={{0,960},{1,57},{8,968},{9,17},{16,976},{17,9},{24,984},{25,33},{32... | collective-permute-start | bytes 1769480 | tf_op jit(solution)/shard_map/ppermute | solution.py:36
  44.3 11.0 %collective-permute-start = (bf16[8,96,384]{2,1,0:T(8,128)(2,1)S(1)}, bf16[8,96,384]{2,1,0:T(8,128)(2,1)S(1)}, u32[]{:S(2)}, u32[]{:S(2)}) collective-permute-start(bf16[8,96,384]{2,1,0:T(8,128)(2,1)S(1)} %all-to-all-done.refs_0_), channel_id=1, source_target_pairs={{0,64},{1,9},{8,72},{9,1},{16,80},{17,25},{24,88},{25,17},{32,96},... | collective-permute-start | bytes 1769480 | tf_op jit(solution)/shard_map/ppermute | solution.py:36
  46.2 37.5 %all-to-all-start.1 = ((bf16[8,64,2048]{2,1,0:T(8,128)(2,1)}), bf16[8,64,2048]{2,1,0:T(8,128)(2,1)}, u32[]{:S(2)}, u32[]{:S(2)}) async-start(bf16[8,64,2048]{2,1,0:T(8,128)(2,1)} %broadcast_in_dim.5), calls=%async_computation.1 | async-start | bytes 4194304 | tf_op jit(solution)/shard_map/all_to_all | solution.py:154
  51.5 11.0 %collective-permute-start.2 = (bf16[8,96,384]{2,1,0:T(8,128)(2,1)S(1)}, bf16[8,96,384]{2,1,0:T(8,128)(2,1)S(1)}, u32[]{:S(2)}, u32[]{:S(2)}) collective-permute-start(bf16[8,96,384]{2,1,0:T(8,128)(2,1)S(1)} %collective-permute-done.1.refs_2_), channel_id=1, source_target_pairs={{0,64},{1,9},{8,72},{9,1},{16,80},{17,25},{24,88},{25,17},{32,96},... | collective-permute-start | bytes 1769480 | tf_op jit(solution)/shard_map/ppermute | solution.py:36
  55.3 12.2 %collective-permute-start.3 = (bf16[8,96,384]{2,1,0:T(8,128)(2,1)S(1)}, bf16[8,96,384]{2,1,0:T(8,128)(2,1)S(1)}, u32[]{:S(2)}, u32[]{:S(2)}) collective-permute-start(bf16[8,96,384]{2,1,0:T(8,128)(2,1)S(1)} %collective-permute-done.refs_1_), channel_id=1, source_target_pairs={{0,960},{1,57},{8,968},{9,17},{16,976},{17,9},{24,984},{25,33},{32... | collective-permute-start | bytes 1769480 | tf_op jit(solution)/shard_map/ppermute | solution.py:36
  62.5 12.2 %collective-permute-start.5 = (bf16[8,96,384]{2,1,0:T(8,128)(2,1)S(1)}, bf16[8,96,384]{2,1,0:T(8,128)(2,1)S(1)}, u32[]{:S(2)}, u32[]{:S(2)}) collective-permute-start(bf16[8,96,384]{2,1,0:T(8,128)(2,1)S(1)} %collective-permute-done.2.refs_3_), channel_id=1, source_target_pairs={{0,960},{1,57},{8,968},{9,17},{16,976},{17,9},{24,984},{25,33},{32... | collective-permute-start | bytes 1769480 | tf_op jit(solution)/shard_map/ppermute | solution.py:36
  67.5 10.9 %copy-start.4 = (bf16[8,96,384]{2,1,0:T(8,128)(2,1)}, bf16[8,96,384]{2,1,0:T(8,128)(2,1)S(1)}, u32[]{:S(2)}) copy-start(bf16[8,96,384]{2,1,0:T(8,128)(2,1)S(1)} %collective-permute-done.3.refs_4_) | copy-start | bytes 1769476
  67.5 10.9 %collective-permute-start.4 = (bf16[8,96,384]{2,1,0:T(8,128)(2,1)S(1)}, bf16[8,96,384]{2,1,0:T(8,128)(2,1)S(1)}, u32[]{:S(2)}, u32[]{:S(2)}) collective-permute-start(bf16[8,96,384]{2,1,0:T(8,128)(2,1)S(1)} %collective-permute-done.3.refs_4_), channel_id=1, source_target_pairs={{0,64},{1,9},{8,72},{9,1},{16,80},{17,25},{24,88},{25,17},{32,96},... | collective-permute-start | bytes 1769480 | tf_op jit(solution)/shard_map/ppermute | solution.py:36
  74.8 0.9 copy-start.6
  76.4 14.6 %collective-permute-start.6 = (bf16[4,96,384]{2,1,0:T(8,128)(2,1)}, bf16[4,96,384]{2,1,0:T(8,128)(2,1)S(1)}, u32[]{:S(2)}, u32[]{:S(2)}) collective-permute-start(bf16[4,96,384]{2,1,0:T(8,128)(2,1)} %slice.8), channel_id=1, source_target_pairs={{0,64},{1,9},{8,72},{9,1},{16,80},{17,25},{24,88},{25,17},{32,96},... | collective-permute-start | bytes 884744 | tf_op jit(solution)/shard_map/ppermute | solution.py:36
  79.2 11.8 %collective-permute-start.7 = (bf16[4,96,384]{2,1,0:T(8,128)(2,1)}, bf16[4,96,384]{2,1,0:T(8,128)(2,1)S(1)}, u32[]{:S(2)}, u32[]{:S(2)}) collective-permute-start(bf16[4,96,384]{2,1,0:T(8,128)(2,1)} %slice.9), channel_id=1, source_target_pairs={{0,960},{1,57},{8,968},{9,17},{16,976},{17,9},{24,984},{25,33},{32... | collective-permute-start | bytes 884744 | tf_op jit(solution)/shard_map/ppermute | solution.py:36
  83.7 1.1 copy-start.5
  90.9 1.4 %copy-start = (f32[2,4,2,64,384]{4,3,2,1,0:T(8,128)S(1)}, f32[2,4,2,64,384]{4,3,2,1,0:T(8,128)}, u32[]{:S(2)}) copy-start(f32[2,4,2,64,384]{4,3,2,1,0:T(8,128)} %get-tuple-element.12.gate_up) | copy-start | bytes 4718596
  92.4 1.4 %copy-start.2 = (bf16[8,8,32,384]{3,2,1,0:T(8,128)(2,1)S(1)}, bf16[8,8,32,384]{3,2,1,0:T(8,128)(2,1)}, u32[]{:S(2)}) copy-start(bf16[8,8,32,384]{3,2,1,0:T(8,128)(2,1)} %get-tuple-element.14.most_down) | copy-start | bytes 4718596
  93.8 6.2 %copy-start.1 = (f32[2,4,2,64,384]{4,3,2,1,0:T(8,128)S(1)}, f32[2,4,2,64,384]{4,3,2,1,0:T(8,128)}, u32[]{:S(2)}) copy-start(f32[2,4,2,64,384]{4,3,2,1,0:T(8,128)} %get-tuple-element.12.gate_up) | copy-start | bytes 4718596
  93.8 6.2 %copy-start.3 = (bf16[8,8,32,384]{3,2,1,0:T(8,128)(2,1)S(1)}, bf16[8,8,32,384]{3,2,1,0:T(8,128)(2,1)}, u32[]{:S(2)}) copy-start(bf16[8,8,32,384]{3,2,1,0:T(8,128)(2,1)} %get-tuple-element.14.most_down) | copy-start | bytes 4718596
  95.5 6.6 %collective-permute-start.8 = (bf16[4,64,2048]{2,1,0:T(8,128)(2,1)S(1)}, bf16[4,64,2048]{2,1,0:T(8,128)(2,1)S(1)}, u32[]{:S(2)}, u32[]{:S(2)}) collective-permute-start(bf16[4,64,2048]{2,1,0:T(8,128)(2,1)S(1)} %shard_map.65), channel_id=1, source_target_pairs={{0,1},{1,0},{2,3},{3,2},{4,5},{5,4},{6,7},{7,6},{8,9},{9,8},{10,11... | collective-permute-start | bytes 3145736 | tf_op jit(solution)/shard_map/ppermute | solution.py:160
  102.5 18.8 %copy-start.9 = (f32[2048]{0:T(1024)S(1)}, f32[2048]{0:T(1024)}, u32[]{:S(2)}) copy-start(f32[2048]{0:T(1024)} %param.11) | copy-start | bytes 24580

commit v2 on v1

--- a/solution.py
+++ b/solution.py
@@ -72,30 +72,25 @@
     x_last[...] = picked.astype(jnp.bfloat16).reshape(4, 2, 64, 256)
 
 
-def last_kernel(ids, gate_up, x_last, most_down, half_0, half_1, out, down):
+def last_kernel(ids, gate_up, x_last, most_down, blk, out, down):
     base, core, which = ids[0], ids[1], ids[2]
     last = (base + 4) & 7
-    halves = (half_0, half_1)
     down[...] = most_down[...]
 
     @pl.when(core == 0)
     def _():
-        for h, half in enumerate(halves):
-            down[last, 4 * h : 4 * h + 4] = half[:, 64:96, :]
+        down[last] = blk[:, 64:96, :]
 
     @pl.when(core == 1)
     def _():
-        for h, half in enumerate(halves):
-            down[4 * h : 4 * h + 4, last] = half[:, 64:96, :]
+        down[:, last] = blk[:, 64:96, :]
 
     x = x_last[:, which].reshape(256, 256)
     sums = []
     for n in range(2):
-        acc = gate_up[n, :, which].reshape(256, 384)
-        for h, half in enumerate(halves):
-            w = half[:, 32 * n : 32 * n + 32, :].reshape(128, 384)
-            acc = acc + jnp.dot(x[:, 128 * h : 128 * h + 128], w, preferred_element_type=jnp.float32)
-        sums.append(acc)
+        w = blk[:, 32 * n : 32 * n + 32, :].reshape(256, 384)
+        rest = jnp.dot(x, w, preferred_element_type=jnp.float32)
+        sums.append(gate_up[n, :, which].reshape(256, 384) + rest)
     gate, up = sums
     hidden = (gate / (1.0 + jnp.exp(-gate)) * up).astype(jnp.bfloat16)
     nt = (((1,), (1,)), ((), ()))
@@ -119,20 +114,20 @@
         in_specs=[SMEM] + [VMEM] * 8,
         out_specs=(VMEM, VMEM, VMEM),
         scratch_shapes=[pltpu.VMEM(WHOLE, jnp.bfloat16)] * 2,
-        compiler_params=pltpu.CompilerParams(vmem_limit_bytes=50 * 1024 * 1024),
+        compiler_params=pltpu.CompilerParams(vmem_limit_bytes=46 * 1024 * 1024),
         name="most",
     )(ids, normed, *blocks)
 
 
-def partial_of(ids, most, halves):
+def partial_of(ids, most, block):
     return pl.pallas_call(
         last_kernel,
         out_shape=jax.ShapeDtypeStruct((4, 64, 2048), jnp.bfloat16),
-        in_specs=[SMEM] + [VMEM] * 5,
+        in_specs=[SMEM] + [VMEM] * 4,
         out_specs=VMEM,
         scratch_shapes=[pltpu.VMEM(WHOLE, jnp.bfloat16)],
         compiler_params=pltpu.CompilerParams(vmem_limit_bytes=16 * 1024 * 1024),
-    )(ids, *most, *halves)
+    )(ids, *most, block)
 
 
 def body(tokens, norm_gain, w_gate, w_up, w_down, post_gain):
@@ -141,7 +136,6 @@
     block = lax.all_to_all(own, PLANE, 0, 0, tiled=True, axis_index_groups=first_groups())
     own_normed = rms_scale(tokens.astype(jnp.float32), norm_gain).astype(jnp.bfloat16)
     copies = jnp.broadcast_to(own_normed[None], (8, *own_normed.shape))
-    block, copies = lax.optimization_barrier((block, copies))
     blocks = [block]
     even = odd = block
     for _ in range(3):
@@ -149,17 +143,16 @@
         odd = exchange(even, 1)
         even = new_even
         blocks += [even, odd]
-    half_0 = exchange(odd[:4], 0)
-    half_1 = exchange(even[4:], 1)
+    final = exchange(odd, 0)
     normed = lax.all_to_all(copies, ("x", "c"), 0, 0, tiled=True)
     core = lax.axis_index("c")
     base = jnp.where(core == 0, lax.axis_index("zl"), lax.axis_index("y"))
     ids = jnp.stack([base, core, 1 - core]).astype(jnp.int32)
     most = most_of(ids, normed, blocks)
-    send = partial_of(ids, most, (half_0, half_1))
+    send = partial_of(ids, most, final)
     other = lax.ppermute(send, "c", [(0, 1), (1, 0)])
     ids = jnp.stack([base, core, core]).astype(jnp.int32)
-    keep = partial_of(ids, most, (half_0, half_1))
+    keep = partial_of(ids, most, final)
     pair = (keep.astype(jnp.float32) + other.astype(jnp.float32)).astype(jnp.bfloat16)
     arrived = lax.all_to_all(pair, "x", split_axis=0, concat_axis=0, tiled=True)
     summed = arrived.astype(jnp.float32).sum(axis=0)

time: 124 us -> 120 us (0.968); the launches traced: 122 us -> 120 us
  waiting for transfers between devices: 29.2 us -> 39.2 us
  local copies, waits for them, and re-layouts: 8.68 us -> 2.44 us
  starting transfers between devices: 53.3 us -> 48.2 us
    ppermute x8 -> x7, waiting for transfers between devices: 12.6 us -> 22.4 us  [exchange(): return lax.ppermute(x, PLANE, pairs)]
    ppermute x8 -> x7, starting transfers between devices: 28.2 us -> 21.9 us  [exchange(): return lax.ppermute(x, PLANE, pairs)]
    unnamed x20 -> x6, local copies, waits for them, and re-layouts: 4.76 us -> 0.01 us
    slice x2 -> x0, local copies, waits for them, and re-layouts: 1.48 us -> none  [the longest x1 0.74 us: body(): half_0 = exchange(odd[:4], 0)]
    ppermute x1, starting transfers between devices: 4.37 us -> 5.65 us  [body(): other = lax.ppermute(send, 'c', [(0, 1), (1, 0)])]
  transfers between devices with their start and end apart: 11 -> 10, of which waited for: 8 -> 8; matrix products, arithmetic and copies ran while one was open for 2% -> 2% of each run, Pallas kernels for 6% -> 6%
where the time goes in v2:
time: 120 us
  starting transfers between devices  48.2 us (40%)
  waiting for transfers between devices  39.2 us (33%)
  blocking collectives  18.6 us (16%)
  Pallas kernels  8.4 us (7%)
  other arithmetic  2.78 us (2%)
  local copies, waits for them, and re-layouts  2.44 us (2%)
    ppermute x7, waiting for transfers between devices, exchange(): return lax.ppermute(x, PLANE, pairs)  22.4 us
    ppermute x7, starting transfers between devices, exchange(): return lax.ppermute(x, PLANE, pairs)  21.9 us
    all_to_all x1, blocking collectives, body(): arrived = lax.all_to_all(pair, 'x', split_axis=0, concat_axis=0, tiled=True)  18.6 us
    all_to_all x1, waiting for transfers between devices, body(): lax.all_to_all(own, PLANE, 0, 0, tiled=True, axis_index_groups=first_grou...  16.3 us
    all_to_all x1, starting transfers between devices, body(): lax.all_to_all(own, PLANE, 0, 0, tiled=True, axis_index_groups=first_grou...  16.2 us
    ppermute x1, starting transfers between devices, body(): other = lax.ppermute(send, 'c', [(0, 1), (1, 0)])  5.65 us
    pallas_call x1, Pallas kernels, most_of(): pl.pallas_call(most_kernel, out_shape=(jax.ShapeDtypeStruct((2, 4, 2, 64,...  5.18 us
    all_to_all x1, starting transfers between devices, body(): normed = lax.all_to_all(copies, ('x', 'c'), 0, 0, tiled=True)  4.41 us
  transfers between devices with their start and end apart: 10, of which 8 were waited for; matrix products, arithmetic and copies ran while one was open for 2% of the time, Pallas kernels for 6%

profile of v2, /device:TPU:1, one launch (start us, length us, event | category | flops | bytes accessed | tf_op | source)
XLA Modules:
  0.0 119.7 jit_solution(10253634569590454905)
XLA Ops:
  0.0 0.0 copy-start
  0.0 0.0 copy-start.1
  0.0 0.8 pad_maximum_fusion
  0.8 0.9 broadcast_in_dim.5
  1.7 16.2 %all-to-all-start.1 = ((bf16[8,96,384]{2,1,0:T(8,128)(2,1)}), bf16[8,96,384]{2,1,0:T(8,128)(2,1)S(1)}, u32[]{:S(2)}, u32[]{:S(2)}) async-start(bf16[8,96,384]{2,1,0:T(8,128)(2,1)} %broadcast_in_dim.5), calls=%async_computation.1 | async-start | bytes 1179648 | tf_op jit(solution)/shard_map/all_to_all | solution.py:136
  17.9 0.0 copy-done
  17.9 0.2 fusion
  18.1 16.3 %all-to-all-done.1.refs_0_ = bf16[8,96,384]{2,1,0:T(8,128)(2,1)S(1)} async-done(((bf16[8,96,384]{2,1,0:T(8,128)(2,1)}), bf16[8,96,384]{2,1,0:T(8,128)(2,1)S(1)}, u32[]{:S(2)}, u32[]{:S(2)}) %all-to-all-start.1) | async-done | bytes 589856 | tf_op jit(solution)/shard_map/all_to_all | solution.py:136
  34.3 8.9 %collective-permute-start.1 = (bf16[8,96,384]{2,1,0:T(8,128)(2,1)S(1)}, bf16[8,96,384]{2,1,0:T(8,128)(2,1)S(1)}, u32[]{:S(2)}, u32[]{:S(2)}) collective-permute-start(bf16[8,96,384]{2,1,0:T(8,128)(2,1)S(1)} %all-to-all-done.1.refs_0_), channel_id=1, source_target_pairs={{0,960},{1,57},{8,968},{9,17},{16,976},{17,9},{24,984},{25,33},{32... | collective-permute-start | bytes 1769480 | tf_op jit(solution)/shard_map/ppermute | solution.py:36
  43.3 0.0 copy-done.1
  43.3 0.1 fusion.2
  43.4 1.6 %broadcast_in_dim.4 = bf16[8,64,2048]{2,1,0:T(8,128)(2,1)} broadcast(bf16[64,2048]{1,0:T(8,128)(2,1)S(1)} %fusion.2), dimensions={1,2} | broadcast | bytes 2359296 | tf_op jit(solution)/shard_map/broadcast_in_dim | solution.py:138
  45.0 4.4 %all-to-all-start = ((bf16[8,64,2048]{2,1,0:T(8,128)(2,1)}), bf16[8,64,2048]{2,1,0:T(8,128)(2,1)}, u32[]{:S(2)}, u32[]{:S(2)}) async-start(bf16[8,64,2048]{2,1,0:T(8,128)(2,1)} %broadcast_in_dim.4), calls=%async_computation | async-start | bytes 4194304 | tf_op jit(solution)/shard_map/all_to_all | solution.py:147
  49.4 1.9 %collective-permute-start = (bf16[8,96,384]{2,1,0:T(8,128)(2,1)S(1)}, bf16[8,96,384]{2,1,0:T(8,128)(2,1)S(1)}, u32[]{:S(2)}, u32[]{:S(2)}) collective-permute-start(bf16[8,96,384]{2,1,0:T(8,128)(2,1)S(1)} %all-to-all-done.1.refs_0_), channel_id=1, source_target_pairs={{0,64},{1,9},{8,72},{9,1},{16,80},{17,25},{24,88},{25,17},{32,96},... | collective-permute-start | bytes 1769480 | tf_op jit(solution)/shard_map/ppermute | solution.py:36
  51.3 0.0 collective-permute-done.1.refs_2_
  51.3 3.4 %collective-permute-start.2 = (bf16[8,96,384]{2,1,0:T(8,128)(2,1)S(1)}, bf16[8,96,384]{2,1,0:T(8,128)(2,1)S(1)}, u32[]{:S(2)}, u32[]{:S(2)}) collective-permute-start(bf16[8,96,384]{2,1,0:T(8,128)(2,1)S(1)} %collective-permute-done.1.refs_2_), channel_id=1, source_target_pairs={{0,64},{1,9},{8,72},{9,1},{16,80},{17,25},{24,88},{25,17},{32,96},... | collective-permute-start | bytes 1769480 | tf_op jit(solution)/shard_map/ppermute | solution.py:36
  54.7 5.7 %collective-permute-done.refs_1_ = bf16[8,96,384]{2,1,0:T(8,128)(2,1)S(1)} collective-permute-done((bf16[8,96,384]{2,1,0:T(8,128)(2,1)S(1)}, bf16[8,96,384]{2,1,0:T(8,128)(2,1)S(1)}, u32[]{:S(2)}, u32[]{:S(2)}) %collective-permute-start) | collective-permute-done | bytes 589856 | tf_op jit(solution)/shard_map/ppermute | solution.py:36
  60.4 1.9 %collective-permute-start.3 = (bf16[8,96,384]{2,1,0:T(8,128)(2,1)S(1)}, bf16[8,96,384]{2,1,0:T(8,128)(2,1)S(1)}, u32[]{:S(2)}, u32[]{:S(2)}) collective-permute-start(bf16[8,96,384]{2,1,0:T(8,128)(2,1)S(1)} %collective-permute-done.refs_1_), channel_id=1, source_target_pairs={{0,960},{1,57},{8,968},{9,17},{16,976},{17,9},{24,984},{25,33},{32... | collective-permute-start | bytes 1769480 | tf_op jit(solution)/shard_map/ppermute | solution.py:36
  62.4 4.4 %collective-permute-done.2.refs_3_ = bf16[8,96,384]{2,1,0:T(8,128)(2,1)S(1)} collective-permute-done((bf16[8,96,384]{2,1,0:T(8,128)(2,1)S(1)}, bf16[8,96,384]{2,1,0:T(8,128)(2,1)S(1)}, u32[]{:S(2)}, u32[]{:S(2)}) %collective-permute-start.2) | collective-permute-done | bytes 589856 | tf_op jit(solution)/shard_map/ppermute | solution.py:36
  66.8 1.9 %collective-permute-start.5 = (bf16[8,96,384]{2,1,0:T(8,128)(2,1)S(1)}, bf16[8,96,384]{2,1,0:T(8,128)(2,1)}, u32[]{:S(2)}, u32[]{:S(2)}) collective-permute-start(bf16[8,96,384]{2,1,0:T(8,128)(2,1)S(1)} %collective-permute-done.2.refs_3_), channel_id=1, source_target_pairs={{0,960},{1,57},{8,968},{9,17},{16,976},{17,9},{24,984},{25,33},{32... | collective-permute-start | bytes 1769480 | tf_op jit(solution)/shard_map/ppermute | solution.py:36
  68.7 4.0 %collective-permute-done.3.refs_4_ = bf16[8,96,384]{2,1,0:T(8,128)(2,1)S(1)} collective-permute-done((bf16[8,96,384]{2,1,0:T(8,128)(2,1)S(1)}, bf16[8,96,384]{2,1,0:T(8,128)(2,1)S(1)}, u32[]{:S(2)}, u32[]{:S(2)}) %collective-permute-start.3) | collective-permute-done | bytes 589856 | tf_op jit(solution)/shard_map/ppermute | solution.py:36
  72.7 1.9 %collective-permute-start.4 = (bf16[8,96,384]{2,1,0:T(8,128)(2,1)S(1)}, bf16[8,96,384]{2,1,0:T(8,128)(2,1)}, u32[]{:S(2)}, u32[]{:S(2)}) collective-permute-start(bf16[8,96,384]{2,1,0:T(8,128)(2,1)S(1)} %collective-permute-done.3.refs_4_), channel_id=1, source_target_pairs={{0,64},{1,9},{8,72},{9,1},{16,80},{17,25},{24,88},{25,17},{32,96},... | collective-permute-start | bytes 1769480 | tf_op jit(solution)/shard_map/ppermute | solution.py:36
  74.6 4.4 %collective-permute-done.5.refs_6_ = bf16[8,96,384]{2,1,0:T(8,128)(2,1)} collective-permute-done((bf16[8,96,384]{2,1,0:T(8,128)(2,1)S(1)}, bf16[8,96,384]{2,1,0:T(8,128)(2,1)}, u32[]{:S(2)}, u32[]{:S(2)}) %collective-permute-start.5) | collective-permute-done | bytes 589856 | tf_op jit(solution)/shard_map/ppermute | solution.py:36
  79.0 1.9 %collective-permute-start.6 = (bf16[8,96,384]{2,1,0:T(8,128)(2,1)}, bf16[8,96,384]{2,1,0:T(8,128)(2,1)S(1)}, u32[]{:S(2)}, u32[]{:S(2)}) collective-permute-start(bf16[8,96,384]{2,1,0:T(8,128)(2,1)} %collective-permute-done.5.refs_6_), channel_id=1, source_target_pairs={{0,64},{1,9},{8,72},{9,1},{16,80},{17,25},{24,88},{25,17},{32,96},... | collective-permute-start | bytes 1769480 | tf_op jit(solution)/shard_map/ppermute | solution.py:36
  80.9 0.1 pad_add_fusion.2.ids
  81.0 0.0 all-to-all-done.normed
  81.0 2.7 %collective-permute-done.4.refs_5_ = bf16[8,96,384]{2,1,0:T(8,128)(2,1)} collective-permute-done((bf16[8,96,384]{2,1,0:T(8,128)(2,1)S(1)}, bf16[8,96,384]{2,1,0:T(8,128)(2,1)}, u32[]{:S(2)}, u32[]{:S(2)}) %collective-permute-start.4) | collective-permute-done | bytes 589856 | tf_op jit(solution)/shard_map/ppermute | solution.py:36
  83.7 5.2 %most.1 = (f32[2,4,2,64,384]{4,3,2,1,0:T(8,128)S(1)}, bf16[4,2,64,256]{3,2,1,0:T(8,128)(2,1)S(1)}, bf16[8,8,32,384]{3,2,1,0:T(8,128)(2,1)S(1)}) custom-call(s32[3]{0:T(128)S(1)} %pad_add_fusion.2.ids, bf16[8,64,2048]{2,1,0:T(8,128)(2,1)} %all-to-all-done.normed, bf16[8,96,384]{2,1,0:T(8,128)(2,1)S(1)} %all-to-all-done.1.refs_0_, ...), custom_call_target="tpu_custom_call" | custom-call | tf_op jit(solution)/shard_map/most/pallas_call | solution.py:107
  88.9 1.2 %collective-permute-done.6.blk = bf16[8,96,384]{2,1,0:T(8,128)(2,1)S(1)} collective-permute-done((bf16[8,96,384]{2,1,0:T(8,128)(2,1)}, bf16[8,96,384]{2,1,0:T(8,128)(2,1)S(1)}, u32[]{:S(2)}, u32[]{:S(2)}) %collective-permute-start.6) | collective-permute-done | bytes 589856 | tf_op jit(solution)/shard_map/ppermute | solution.py:36
  90.1 1.6 %shard_map.65 = bf16[4,64,2048]{2,1,0:T(8,128)(2,1)S(1)} custom-call(s32[3]{0:T(128)S(1)} %pad_add_fusion.2.ids, f32[2,4,2,64,384]{4,3,2,1,0:T(8,128)S(1)} %get-tuple-element.8.gate_up, bf16[4,2,64,256]{3,2,1,0:T(8,128)(2,1)S(1)} %get-tuple-element.9.x_last, bf16[8,8,32,384]{3,2,1,0:T(8,128)(2,1)S(1)} %get-tuple-element.10.most_down, ...), custom_call_target="tpu_custom_call" | custom-call | tf_op jit(solution)/shard_map/pallas_call | solution.py:123
  91.7 5.6 %collective-permute-start.7 = (bf16[4,64,2048]{2,1,0:T(8,128)(2,1)S(1)}, bf16[4,64,2048]{2,1,0:T(8,128)(2,1)S(1)}, u32[]{:S(2)}, u32[]{:S(2)}) collective-permute-start(bf16[4,64,2048]{2,1,0:T(8,128)(2,1)S(1)} %shard_map.65), channel_id=1, source_target_pairs={{0,1},{1,0},{2,3},{3,2},{4,5},{5,4},{6,7},{7,6},{8,9},{9,8},{10,11... | collective-permute-start | bytes 3145736 | tf_op jit(solution)/shard_map/ppermute | solution.py:153
  97.4 0.1 pad_add_fusion.ids
  97.4 1.6 %shard_map.64 = bf16[4,64,2048]{2,1,0:T(8,128)(2,1)S(1)} custom-call(s32[3]{0:T(128)S(1)} %pad_add_fusion.ids, f32[2,4,2,64,384]{4,3,2,1,0:T(8,128)S(1)} %get-tuple-element.8.gate_up, bf16[4,2,64,256]{3,2,1,0:T(8,128)(2,1)S(1)} %get-tuple-element.9.x_last, bf16[8,8,32,384]{3,2,1,0:T(8,128)(2,1)S(1)} %get-tuple-element.10.most_down, ...), custom_call_target="tpu_custom_call" | custom-call | tf_op jit(solution)/shard_map/pallas_call | solution.py:123
  99.1 0.6 collective-permute-done.7
  99.6 0.4 add_convert_fusion
  100.0 0.0 copy-start.2
  100.0 18.6 %all_to_all.15 = bf16[4,64,2048]{2,1,0:T(8,128)(2,1)S(1)} all-to-all(bf16[4,64,2048]{2,1,0:T(8,128)(2,1)S(1)} %add_convert_fusion), channel_id=1, replica_groups=mesh['zh'=2,'zl'=8,'y'=8,'x'=4,'c'=2] {'x'}, dimensions={0} | all-to-all | bytes 2097152 | tf_op jit(solution)/shard_map/all_to_all | solution.py:157
  118.6 0.2 convert_reduce_fusion
  118.8 0.1 multiply_reduce_fusion
  118.9 0.0 copy-done.2
  118.9 0.8 multiply_convert_fusion
  (2 shorter events, 0.0 us)
Async XLA Ops:
  0.0 17.9 %copy-start = (bf16[64,2048]{1,0:T(8,128)(2,1)S(1)}, bf16[64,2048]{1,0:T(8,128)(2,1)}, u32[]{:S(2)}) copy-start(bf16[64,2048]{1,0:T(8,128)(2,1)} %param.6) | copy-start | bytes 786436
  0.0 43.3 %copy-start.1 = (f32[2048]{0:T(1024)S(1)}, f32[2048]{0:T(1024)}, u32[]{:S(2)}) copy-start(f32[2048]{0:T(1024)} %param.7) | copy-start | bytes 24580
  1.7 32.7 %all-to-all-start.1 = ((bf16[8,96,384]{2,1,0:T(8,128)(2,1)}), bf16[8,96,384]{2,1,0:T(8,128)(2,1)S(1)}, u32[]{:S(2)}, u32[]{:S(2)}) async-start(bf16[8,96,384]{2,1,0:T(8,128)(2,1)} %broadcast_in_dim.5), calls=%async_computation.1 | async-start | bytes 1179648 | tf_op jit(solution)/shard_map/all_to_all | solution.py:136
  34.3 17.0 %collective-permute-start.1 = (bf16[8,96,384]{2,1,0:T(8,128)(2,1)S(1)}, bf16[8,96,384]{2,1,0:T(8,128)(2,1)S(1)}, u32[]{:S(2)}, u32[]{:S(2)}) collective-permute-start(bf16[8,96,384]{2,1,0:T(8,128)(2,1)S(1)} %all-to-all-done.1.refs_0_), channel_id=1, source_target_pairs={{0,960},{1,57},{8,968},{9,17},{16,976},{17,9},{24,984},{25,33},{32... | collective-permute-start | bytes 1769480 | tf_op jit(solution)/shard_map/ppermute | solution.py:36
  45.0 36.0 %all-to-all-start = ((bf16[8,64,2048]{2,1,0:T(8,128)(2,1)}), bf16[8,64,2048]{2,1,0:T(8,128)(2,1)}, u32[]{:S(2)}, u32[]{:S(2)}) async-start(bf16[8,64,2048]{2,1,0:T(8,128)(2,1)} %broadcast_in_dim.4), calls=%async_computation | async-start | bytes 4194304 | tf_op jit(solution)/shard_map/all_to_all | solution.py:147
  49.4 11.0 %collective-permute-start = (bf16[8,96,384]{2,1,0:T(8,128)(2,1)S(1)}, bf16[8,96,384]{2,1,0:T(8,128)(2,1)S(1)}, u32[]{:S(2)}, u32[]{:S(2)}) collective-permute-start(bf16[8,96,384]{2,1,0:T(8,128)(2,1)S(1)} %all-to-all-done.1.refs_0_), channel_id=1, source_target_pairs={{0,64},{1,9},{8,72},{9,1},{16,80},{17,25},{24,88},{25,17},{32,96},... | collective-permute-start | bytes 1769480 | tf_op jit(solution)/shard_map/ppermute | solution.py:36
  51.3 15.4 %collective-permute-start.2 = (bf16[8,96,384]{2,1,0:T(8,128)(2,1)S(1)}, bf16[8,96,384]{2,1,0:T(8,128)(2,1)S(1)}, u32[]{:S(2)}, u32[]{:S(2)}) collective-permute-start(bf16[8,96,384]{2,1,0:T(8,128)(2,1)S(1)} %collective-permute-done.1.refs_2_), channel_id=1, source_target_pairs={{0,64},{1,9},{8,72},{9,1},{16,80},{17,25},{24,88},{25,17},{32,96},... | collective-permute-start | bytes 1769480 | tf_op jit(solution)/shard_map/ppermute | solution.py:36
  60.4 12.2 %collective-permute-start.3 = (bf16[8,96,384]{2,1,0:T(8,128)(2,1)S(1)}, bf16[8,96,384]{2,1,0:T(8,128)(2,1)S(1)}, u32[]{:S(2)}, u32[]{:S(2)}) collective-permute-start(bf16[8,96,384]{2,1,0:T(8,128)(2,1)S(1)} %collective-permute-done.refs_1_), channel_id=1, source_target_pairs={{0,960},{1,57},{8,968},{9,17},{16,976},{17,9},{24,984},{25,33},{32... | collective-permute-start | bytes 1769480 | tf_op jit(solution)/shard_map/ppermute | solution.py:36
  66.8 12.2 %collective-permute-start.5 = (bf16[8,96,384]{2,1,0:T(8,128)(2,1)S(1)}, bf16[8,96,384]{2,1,0:T(8,128)(2,1)}, u32[]{:S(2)}, u32[]{:S(2)}) collective-permute-start(bf16[8,96,384]{2,1,0:T(8,128)(2,1)S(1)} %collective-permute-done.2.refs_3_), channel_id=1, source_target_pairs={{0,960},{1,57},{8,968},{9,17},{16,976},{17,9},{24,984},{25,33},{32... | collective-permute-start | bytes 1769480 | tf_op jit(solution)/shard_map/ppermute | solution.py:36
  72.7 11.0 %collective-permute-start.4 = (bf16[8,96,384]{2,1,0:T(8,128)(2,1)S(1)}, bf16[8,96,384]{2,1,0:T(8,128)(2,1)}, u32[]{:S(2)}, u32[]{:S(2)}) collective-permute-start(bf16[8,96,384]{2,1,0:T(8,128)(2,1)S(1)} %collective-permute-done.3.refs_4_), channel_id=1, source_target_pairs={{0,64},{1,9},{8,72},{9,1},{16,80},{17,25},{24,88},{25,17},{32,96},... | collective-permute-start | bytes 1769480 | tf_op jit(solution)/shard_map/ppermute | solution.py:36
  79.0 11.1 %collective-permute-start.6 = (bf16[8,96,384]{2,1,0:T(8,128)(2,1)}, bf16[8,96,384]{2,1,0:T(8,128)(2,1)S(1)}, u32[]{:S(2)}, u32[]{:S(2)}) collective-permute-start(bf16[8,96,384]{2,1,0:T(8,128)(2,1)} %collective-permute-done.5.refs_6_), channel_id=1, source_target_pairs={{0,64},{1,9},{8,72},{9,1},{16,80},{17,25},{24,88},{25,17},{32,96},... | collective-permute-start | bytes 1769480 | tf_op jit(solution)/shard_map/ppermute | solution.py:36
  91.7 7.9 %collective-permute-start.7 = (bf16[4,64,2048]{2,1,0:T(8,128)(2,1)S(1)}, bf16[4,64,2048]{2,1,0:T(8,128)(2,1)S(1)}, u32[]{:S(2)}, u32[]{:S(2)}) collective-permute-start(bf16[4,64,2048]{2,1,0:T(8,128)(2,1)S(1)} %shard_map.65), channel_id=1, source_target_pairs={{0,1},{1,0},{2,3},{3,2},{4,5},{5,4},{6,7},{7,6},{8,9},{9,8},{10,11... | collective-permute-start | bytes 3145736 | tf_op jit(solution)/shard_map/ppermute | solution.py:153
  100.0 18.9 %copy-start.2 = (f32[2048]{0:T(1024)S(1)}, f32[2048]{0:T(1024)}, u32[]{:S(2)}) copy-start(f32[2048]{0:T(1024)} %param.11) | copy-start | bytes 24580

commit v3 on v2

--- a/solution.py
+++ b/solution.py
@@ -95,7 +95,9 @@
     hidden = (gate / (1.0 + jnp.exp(-gate)) * up).astype(jnp.bfloat16)
     nt = (((1,), (1,)), ((), ()))
     part = lax.dot_general(hidden, down[...].reshape(2048, 384), nt, preferred_element_type=jnp.float32)
-    out[...] = part.astype(jnp.bfloat16).reshape(4, 64, 2048)
+    part = part.astype(jnp.bfloat16)
+    for k in range(4):
+        out[ids[3] ^ k] = part[64 * k : 64 * k + 64]
 
 
 VMEM = pl.BlockSpec(memory_space=pltpu.VMEM)
@@ -145,17 +147,19 @@
         blocks += [even, odd]
     final = exchange(odd, 0)
     normed = lax.all_to_all(copies, ("x", "c"), 0, 0, tiled=True)
-    core = lax.axis_index("c")
+    core, col = lax.axis_index("c"), lax.axis_index("x")
     base = jnp.where(core == 0, lax.axis_index("zl"), lax.axis_index("y"))
-    ids = jnp.stack([base, core, 1 - core]).astype(jnp.int32)
+    ids = jnp.stack([base, core, 1 - core, col]).astype(jnp.int32)
     most = most_of(ids, normed, blocks)
     send = partial_of(ids, most, final)
     other = lax.ppermute(send, "c", [(0, 1), (1, 0)])
-    ids = jnp.stack([base, core, core]).astype(jnp.int32)
+    ids = jnp.stack([base, core, core, col]).astype(jnp.int32)
     keep = partial_of(ids, most, final)
-    pair = (keep.astype(jnp.float32) + other.astype(jnp.float32)).astype(jnp.bfloat16)
-    arrived = lax.all_to_all(pair, "x", split_axis=0, concat_axis=0, tiled=True)
-    summed = arrived.astype(jnp.float32).sum(axis=0)
+    pair = [keep[k].astype(jnp.float32) + other[k].astype(jnp.float32) for k in range(4)]
+    summed = pair[0]
+    for k in (2, 1, 3):
+        got = lax.ppermute(pair[k].astype(jnp.bfloat16), "x", [(x, x ^ k) for x in range(4)])
+        summed = summed + got.astype(jnp.float32)
     return rms_scale(summed, post_gain).astype(jnp.bfloat16)
 
 

time: 120 us -> 121 us (level)
  blocking collectives: 18.6 us -> 0 us
  waiting for transfers between devices: 39.2 us -> 49 us
  starting transfers between devices: 48.2 us -> 57.4 us
    all_to_all x1 -> x0, blocking collectives: 18.6 us -> none  [body(): arrived = lax.all_to_all(pair, 'x', split_axis=0, concat_axis=0, tiled=True)]
    ppermute x0 -> x3, waiting for transfers between devices: none -> 9.75 us  [body(): lax.ppermute(pair[k].astype(jnp.bfloat16), 'x', [(x, x ^ k) for x in rang...]
    ppermute x0 -> x3, starting transfers between devices: none -> 9.27 us  [body(): lax.ppermute(pair[k].astype(jnp.bfloat16), 'x', [(x, x ^ k) for x in rang...]
  transfers between devices with their start and end apart: 10 -> 13, of which waited for: 8 -> 10; matrix products, arithmetic and copies ran while one was open for 2% -> 2% of each run, Pallas kernels for 6% -> 6%
where the time goes in v3:
time: 121 us; the launch traced here: 120 us
  starting transfers between devices  57.4 us (47%)
  waiting for transfers between devices  49 us (40%)
  Pallas kernels  8.41 us (7%)
  other arithmetic  2.75 us (2%)
  local copies, waits for them, and re-layouts  2.47 us (2%)
    ppermute x7, waiting for transfers between devices, exchange(): return lax.ppermute(x, PLANE, pairs)  22.4 us
    ppermute x7, starting transfers between devices, exchange(): return lax.ppermute(x, PLANE, pairs)  21.9 us
    all_to_all x1, waiting for transfers between devices, body(): lax.all_to_all(own, PLANE, 0, 0, tiled=True, axis_index_groups=first_grou...  16.3 us
    all_to_all x1, starting transfers between devices, body(): lax.all_to_all(own, PLANE, 0, 0, tiled=True, axis_index_groups=first_grou...  16.2 us
    ppermute x3, waiting for transfers between devices, body(): lax.ppermute(pair[k].astype(jnp.bfloat16), 'x', [(x, x ^ k) for x in rang...  9.75 us
    ppermute x3, starting transfers between devices, body(): lax.ppermute(pair[k].astype(jnp.bfloat16), 'x', [(x, x ^ k) for x in rang...  9.27 us
    ppermute x1, starting transfers between devices, body(): other = lax.ppermute(send, 'c', [(0, 1), (1, 0)])  5.65 us
    pallas_call x1, Pallas kernels, most_of(): pl.pallas_call(most_kernel, out_shape=(jax.ShapeDtypeStruct((2, 4, 2, 64,...  5.18 us
  transfers between devices with their start and end apart: 13, of which 10 were waited for; matrix products, arithmetic and copies ran while one was open for 2% of the time, Pallas kernels for 6%

profile of v3, /device:TPU:1, one launch (start us, length us, event | category | flops | bytes accessed | tf_op | source)
XLA Modules:
  0.0 120.2 jit_solution(17573903863615160653)
XLA Ops:
  0.0 0.0 copy-start
  0.0 0.0 copy-start.1
  0.0 0.8 pad_maximum_fusion
  0.8 0.9 broadcast_in_dim.5
  1.7 16.2 %all-to-all-start.1 = ((bf16[8,96,384]{2,1,0:T(8,128)(2,1)}), bf16[8,96,384]{2,1,0:T(8,128)(2,1)S(1)}, u32[]{:S(2)}, u32[]{:S(2)}) async-start(bf16[8,96,384]{2,1,0:T(8,128)(2,1)} %broadcast_in_dim.5), calls=%async_computation.1 | async-start | bytes 1179648 | tf_op jit(solution)/shard_map/all_to_all | solution.py:138
  17.9 0.0 copy-done
  18.0 0.2 fusion
  18.1 16.3 %all-to-all-done.1.refs_0_ = bf16[8,96,384]{2,1,0:T(8,128)(2,1)S(1)} async-done(((bf16[8,96,384]{2,1,0:T(8,128)(2,1)}), bf16[8,96,384]{2,1,0:T(8,128)(2,1)S(1)}, u32[]{:S(2)}, u32[]{:S(2)}) %all-to-all-start.1) | async-done | bytes 589856 | tf_op jit(solution)/shard_map/all_to_all | solution.py:138
  34.4 8.9 %collective-permute-start.1 = (bf16[8,96,384]{2,1,0:T(8,128)(2,1)S(1)}, bf16[8,96,384]{2,1,0:T(8,128)(2,1)S(1)}, u32[]{:S(2)}, u32[]{:S(2)}) collective-permute-start(bf16[8,96,384]{2,1,0:T(8,128)(2,1)S(1)} %all-to-all-done.1.refs_0_), channel_id=1, source_target_pairs={{0,960},{1,57},{8,968},{9,17},{16,976},{17,9},{24,984},{25,33},{32... | collective-permute-start | bytes 1769480 | tf_op jit(solution)/shard_map/ppermute | solution.py:36
  43.3 0.0 copy-done.1
  43.3 0.1 fusion.2
  43.5 1.6 %broadcast_in_dim.4 = bf16[8,64,2048]{2,1,0:T(8,128)(2,1)} broadcast(bf16[64,2048]{1,0:T(8,128)(2,1)S(1)} %fusion.2), dimensions={1,2} | broadcast | bytes 2359296 | tf_op jit(solution)/shard_map/broadcast_in_dim | solution.py:140
  45.0 4.4 %all-to-all-start = ((bf16[8,64,2048]{2,1,0:T(8,128)(2,1)}), bf16[8,64,2048]{2,1,0:T(8,128)(2,1)}, u32[]{:S(2)}, u32[]{:S(2)}) async-start(bf16[8,64,2048]{2,1,0:T(8,128)(2,1)} %broadcast_in_dim.4), calls=%async_computation | async-start | bytes 4194304 | tf_op jit(solution)/shard_map/all_to_all | solution.py:149
  49.4 1.9 %collective-permute-start = (bf16[8,96,384]{2,1,0:T(8,128)(2,1)S(1)}, bf16[8,96,384]{2,1,0:T(8,128)(2,1)S(1)}, u32[]{:S(2)}, u32[]{:S(2)}) collective-permute-start(bf16[8,96,384]{2,1,0:T(8,128)(2,1)S(1)} %all-to-all-done.1.refs_0_), channel_id=1, source_target_pairs={{0,64},{1,9},{8,72},{9,1},{16,80},{17,25},{24,88},{25,17},{32,96},... | collective-permute-start | bytes 1769480 | tf_op jit(solution)/shard_map/ppermute | solution.py:36
  51.4 0.0 collective-permute-done.1.refs_2_
  51.4 3.4 %collective-permute-start.2 = (bf16[8,96,384]{2,1,0:T(8,128)(2,1)S(1)}, bf16[8,96,384]{2,1,0:T(8,128)(2,1)S(1)}, u32[]{:S(2)}, u32[]{:S(2)}) collective-permute-start(bf16[8,96,384]{2,1,0:T(8,128)(2,1)S(1)} %collective-permute-done.1.refs_2_), channel_id=1, source_target_pairs={{0,64},{1,9},{8,72},{9,1},{16,80},{17,25},{24,88},{25,17},{32,96},... | collective-permute-start | bytes 1769480 | tf_op jit(solution)/shard_map/ppermute | solution.py:36
  54.7 5.7 %collective-permute-done.refs_1_ = bf16[8,96,384]{2,1,0:T(8,128)(2,1)S(1)} collective-permute-done((bf16[8,96,384]{2,1,0:T(8,128)(2,1)S(1)}, bf16[8,96,384]{2,1,0:T(8,128)(2,1)S(1)}, u32[]{:S(2)}, u32[]{:S(2)}) %collective-permute-start) | collective-permute-done | bytes 589856 | tf_op jit(solution)/shard_map/ppermute | solution.py:36
  60.5 1.9 %collective-permute-start.3 = (bf16[8,96,384]{2,1,0:T(8,128)(2,1)S(1)}, bf16[8,96,384]{2,1,0:T(8,128)(2,1)S(1)}, u32[]{:S(2)}, u32[]{:S(2)}) collective-permute-start(bf16[8,96,384]{2,1,0:T(8,128)(2,1)S(1)} %collective-permute-done.refs_1_), channel_id=1, source_target_pairs={{0,960},{1,57},{8,968},{9,17},{16,976},{17,9},{24,984},{25,33},{32... | collective-permute-start | bytes 1769480 | tf_op jit(solution)/shard_map/ppermute | solution.py:36
  62.4 4.4 %collective-permute-done.2.refs_3_ = bf16[8,96,384]{2,1,0:T(8,128)(2,1)S(1)} collective-permute-done((bf16[8,96,384]{2,1,0:T(8,128)(2,1)S(1)}, bf16[8,96,384]{2,1,0:T(8,128)(2,1)S(1)}, u32[]{:S(2)}, u32[]{:S(2)}) %collective-permute-start.2) | collective-permute-done | bytes 589856 | tf_op jit(solution)/shard_map/ppermute | solution.py:36
  66.8 1.9 %collective-permute-start.5 = (bf16[8,96,384]{2,1,0:T(8,128)(2,1)S(1)}, bf16[8,96,384]{2,1,0:T(8,128)(2,1)}, u32[]{:S(2)}, u32[]{:S(2)}) collective-permute-start(bf16[8,96,384]{2,1,0:T(8,128)(2,1)S(1)} %collective-permute-done.2.refs_3_), channel_id=1, source_target_pairs={{0,960},{1,57},{8,968},{9,17},{16,976},{17,9},{24,984},{25,33},{32... | collective-permute-start | bytes 1769480 | tf_op jit(solution)/shard_map/ppermute | solution.py:36
  68.7 4.0 %collective-permute-done.3.refs_4_ = bf16[8,96,384]{2,1,0:T(8,128)(2,1)S(1)} collective-permute-done((bf16[8,96,384]{2,1,0:T(8,128)(2,1)S(1)}, bf16[8,96,384]{2,1,0:T(8,128)(2,1)S(1)}, u32[]{:S(2)}, u32[]{:S(2)}) %collective-permute-start.3) | collective-permute-done | bytes 589856 | tf_op jit(solution)/shard_map/ppermute | solution.py:36
  72.7 1.9 %collective-permute-start.4 = (bf16[8,96,384]{2,1,0:T(8,128)(2,1)S(1)}, bf16[8,96,384]{2,1,0:T(8,128)(2,1)}, u32[]{:S(2)}, u32[]{:S(2)}) collective-permute-start(bf16[8,96,384]{2,1,0:T(8,128)(2,1)S(1)} %collective-permute-done.3.refs_4_), channel_id=1, source_target_pairs={{0,64},{1,9},{8,72},{9,1},{16,80},{17,25},{24,88},{25,17},{32,96},... | collective-permute-start | bytes 1769480 | tf_op jit(solution)/shard_map/ppermute | solution.py:36
  74.6 4.4 %collective-permute-done.5.refs_6_ = bf16[8,96,384]{2,1,0:T(8,128)(2,1)} collective-permute-done((bf16[8,96,384]{2,1,0:T(8,128)(2,1)S(1)}, bf16[8,96,384]{2,1,0:T(8,128)(2,1)}, u32[]{:S(2)}, u32[]{:S(2)}) %collective-permute-start.5) | collective-permute-done | bytes 589856 | tf_op jit(solution)/shard_map/ppermute | solution.py:36
  79.0 1.9 %collective-permute-start.6 = (bf16[8,96,384]{2,1,0:T(8,128)(2,1)}, bf16[8,96,384]{2,1,0:T(8,128)(2,1)S(1)}, u32[]{:S(2)}, u32[]{:S(2)}) collective-permute-start(bf16[8,96,384]{2,1,0:T(8,128)(2,1)} %collective-permute-done.5.refs_6_), channel_id=1, source_target_pairs={{0,64},{1,9},{8,72},{9,1},{16,80},{17,25},{24,88},{25,17},{32,96},... | collective-permute-start | bytes 1769480 | tf_op jit(solution)/shard_map/ppermute | solution.py:36
  80.9 0.1 add_add_fusion.1.ids
  81.0 0.0 all-to-all-done.normed
  81.0 2.7 %collective-permute-done.4.refs_5_ = bf16[8,96,384]{2,1,0:T(8,128)(2,1)} collective-permute-done((bf16[8,96,384]{2,1,0:T(8,128)(2,1)S(1)}, bf16[8,96,384]{2,1,0:T(8,128)(2,1)}, u32[]{:S(2)}, u32[]{:S(2)}) %collective-permute-start.4) | collective-permute-done | bytes 589856 | tf_op jit(solution)/shard_map/ppermute | solution.py:36
  83.7 5.2 %most.1 = (f32[2,4,2,64,384]{4,3,2,1,0:T(8,128)S(1)}, bf16[4,2,64,256]{3,2,1,0:T(8,128)(2,1)S(1)}, bf16[8,8,32,384]{3,2,1,0:T(8,128)(2,1)S(1)}) custom-call(s32[4]{0:T(128)S(1)} %add_add_fusion.1.ids, bf16[8,64,2048]{2,1,0:T(8,128)(2,1)} %all-to-all-done.normed, bf16[8,96,384]{2,1,0:T(8,128)(2,1)S(1)} %all-to-all-done.1.refs_0_, ...), custom_call_target="tpu_custom_call" | custom-call | tf_op jit(solution)/shard_map/most/pallas_call | solution.py:109
  88.9 1.2 %collective-permute-done.6.blk = bf16[8,96,384]{2,1,0:T(8,128)(2,1)S(1)} collective-permute-done((bf16[8,96,384]{2,1,0:T(8,128)(2,1)}, bf16[8,96,384]{2,1,0:T(8,128)(2,1)S(1)}, u32[]{:S(2)}, u32[]{:S(2)}) %collective-permute-start.6) | collective-permute-done | bytes 589856 | tf_op jit(solution)/shard_map/ppermute | solution.py:36
  90.1 1.6 %shard_map.65 = bf16[4,64,2048]{2,1,0:T(8,128)(2,1)S(1)} custom-call(s32[4]{0:T(128)S(1)} %add_add_fusion.1.ids, f32[2,4,2,64,384]{4,3,2,1,0:T(8,128)S(1)} %get-tuple-element.8.gate_up, bf16[4,2,64,256]{3,2,1,0:T(8,128)(2,1)S(1)} %get-tuple-element.9.x_last, bf16[8,8,32,384]{3,2,1,0:T(8,128)(2,1)S(1)} %get-tuple-element.10.most_down, ...), custom_call_target="tpu_custom_call" | custom-call | tf_op jit(solution)/shard_map/pallas_call | solution.py:125
  91.8 5.6 %collective-permute-start.7 = (bf16[4,64,2048]{2,1,0:T(8,128)(2,1)S(1)}, bf16[4,64,2048]{2,1,0:T(8,128)(2,1)S(1)}, u32[]{:S(2)}, u32[]{:S(2)}) collective-permute-start(bf16[4,64,2048]{2,1,0:T(8,128)(2,1)S(1)} %shard_map.65), channel_id=1, source_target_pairs={{0,1},{1,0},{2,3},{3,2},{4,5},{5,4},{6,7},{7,6},{8,9},{9,8},{10,11... | collective-permute-start | bytes 3145736 | tf_op jit(solution)/shard_map/ppermute | solution.py:155
  97.4 0.1 add_add_fusion.ids
  97.5 1.6 %shard_map.64 = bf16[4,64,2048]{2,1,0:T(8,128)(2,1)S(1)} custom-call(s32[4]{0:T(128)S(1)} %add_add_fusion.ids, f32[2,4,2,64,384]{4,3,2,1,0:T(8,128)S(1)} %get-tuple-element.8.gate_up, bf16[4,2,64,256]{3,2,1,0:T(8,128)(2,1)S(1)} %get-tuple-element.9.x_last, bf16[8,8,32,384]{3,2,1,0:T(8,128)(2,1)S(1)} %get-tuple-element.10.most_down, ...), custom_call_target="tpu_custom_call" | custom-call | tf_op jit(solution)/shard_map/pallas_call | solution.py:125
  99.1 0.0 copy-start.2
  99.1 0.5 collective-permute-done.7
  99.7 0.3 fusion.5
  99.9 4.9 %collective-permute-start.10 = (bf16[64,2048]{1,0:T(8,128)(2,1)S(1)}, bf16[64,2048]{1,0:T(8,128)(2,1)S(1)}, u32[]{:S(2)}, u32[]{:S(2)}) collective-permute-start(bf16[64,2048]{1,0:T(8,128)(2,1)S(1)} %get-tuple-element.12), channel_id=1, source_target_pairs={{0,6},{2,4},{4,2},{6,0},{1,7},{3,5},{5,3},{7,1},{8,14},{10,12},{12... | collective-permute-start | bytes 786440 | tf_op jit(solution)/shard_map/ppermute | solution.py:161
  104.8 2.5 %collective-permute-start.8 = (bf16[64,2048]{1,0:T(8,128)(2,1)S(1)}, bf16[64,2048]{1,0:T(8,128)(2,1)S(1)}, u32[]{:S(2)}, u32[]{:S(2)}) collective-permute-start(bf16[64,2048]{1,0:T(8,128)(2,1)S(1)} %get-tuple-element.11), channel_id=1, source_target_pairs={{0,4},{2,6},{4,0},{6,2},{1,5},{3,7},{5,1},{7,3},{8,12},{10,14},{12... | collective-permute-start | bytes 786440 | tf_op jit(solution)/shard_map/ppermute | solution.py:161
  107.3 1.9 %collective-permute-start.9 = (bf16[64,2048]{1,0:T(8,128)(2,1)S(1)}, bf16[64,2048]{1,0:T(8,128)(2,1)S(1)}, u32[]{:S(2)}, u32[]{:S(2)}) collective-permute-start(bf16[64,2048]{1,0:T(8,128)(2,1)S(1)} %get-tuple-element.13), channel_id=1, source_target_pairs={{0,2},{2,0},{4,6},{6,4},{1,3},{3,1},{5,7},{7,5},{8,10},{10,8},{12,... | collective-permute-start | bytes 786440 | tf_op jit(solution)/shard_map/ppermute | solution.py:161
  109.2 6.6 %collective-permute-done.10 = bf16[64,2048]{1,0:T(8,128)(2,1)S(1)} collective-permute-done((bf16[64,2048]{1,0:T(8,128)(2,1)S(1)}, bf16[64,2048]{1,0:T(8,128)(2,1)S(1)}, u32[]{:S(2)}, u32[]{:S(2)}) %collective-permute-start.10) | collective-permute-done | bytes 262176 | tf_op jit(solution)/shard_map/ppermute | solution.py:161
  115.8 0.0 collective-permute-done.8
  115.8 3.2 %collective-permute-done.9 = bf16[64,2048]{1,0:T(8,128)(2,1)S(1)} collective-permute-done((bf16[64,2048]{1,0:T(8,128)(2,1)S(1)}, bf16[64,2048]{1,0:T(8,128)(2,1)S(1)}, u32[]{:S(2)}, u32[]{:S(2)}) %collective-permute-start.9) | collective-permute-done | bytes 262176 | tf_op jit(solution)/shard_map/ppermute | solution.py:161
  119.0 0.3 multiply_reduce_fusion
  119.3 0.0 copy-done.2
  119.3 0.9 multiply_convert_fusion
  (2 shorter events, 0.0 us)
Async XLA Ops:
  0.0 17.9 %copy-start = (bf16[64,2048]{1,0:T(8,128)(2,1)S(1)}, bf16[64,2048]{1,0:T(8,128)(2,1)}, u32[]{:S(2)}) copy-start(bf16[64,2048]{1,0:T(8,128)(2,1)} %param.6) | copy-start | bytes 786436
  0.0 43.3 %copy-start.1 = (f32[2048]{0:T(1024)S(1)}, f32[2048]{0:T(1024)}, u32[]{:S(2)}) copy-start(f32[2048]{0:T(1024)} %param.7) | copy-start | bytes 24580
  1.7 32.7 %all-to-all-start.1 = ((bf16[8,96,384]{2,1,0:T(8,128)(2,1)}), bf16[8,96,384]{2,1,0:T(8,128)(2,1)S(1)}, u32[]{:S(2)}, u32[]{:S(2)}) async-start(bf16[8,96,384]{2,1,0:T(8,128)(2,1)} %broadcast_in_dim.5), calls=%async_computation.1 | async-start | bytes 1179648 | tf_op jit(solution)/shard_map/all_to_all | solution.py:138
  34.4 17.0 %collective-permute-start.1 = (bf16[8,96,384]{2,1,0:T(8,128)(2,1)S(1)}, bf16[8,96,384]{2,1,0:T(8,128)(2,1)S(1)}, u32[]{:S(2)}, u32[]{:S(2)}) collective-permute-start(bf16[8,96,384]{2,1,0:T(8,128)(2,1)S(1)} %all-to-all-done.1.refs_0_), channel_id=1, source_target_pairs={{0,960},{1,57},{8,968},{9,17},{16,976},{17,9},{24,984},{25,33},{32... | collective-permute-start | bytes 1769480 | tf_op jit(solution)/shard_map/ppermute | solution.py:36
  45.0 36.0 %all-to-all-start = ((bf16[8,64,2048]{2,1,0:T(8,128)(2,1)}), bf16[8,64,2048]{2,1,0:T(8,128)(2,1)}, u32[]{:S(2)}, u32[]{:S(2)}) async-start(bf16[8,64,2048]{2,1,0:T(8,128)(2,1)} %broadcast_in_dim.4), calls=%async_computation | async-start | bytes 4194304 | tf_op jit(solution)/shard_map/all_to_all | solution.py:149
  49.4 11.0 %collective-permute-start = (bf16[8,96,384]{2,1,0:T(8,128)(2,1)S(1)}, bf16[8,96,384]{2,1,0:T(8,128)(2,1)S(1)}, u32[]{:S(2)}, u32[]{:S(2)}) collective-permute-start(bf16[8,96,384]{2,1,0:T(8,128)(2,1)S(1)} %all-to-all-done.1.refs_0_), channel_id=1, source_target_pairs={{0,64},{1,9},{8,72},{9,1},{16,80},{17,25},{24,88},{25,17},{32,96},... | collective-permute-start | bytes 1769480 | tf_op jit(solution)/shard_map/ppermute | solution.py:36
  51.4 15.4 %collective-permute-start.2 = (bf16[8,96,384]{2,1,0:T(8,128)(2,1)S(1)}, bf16[8,96,384]{2,1,0:T(8,128)(2,1)S(1)}, u32[]{:S(2)}, u32[]{:S(2)}) collective-permute-start(bf16[8,96,384]{2,1,0:T(8,128)(2,1)S(1)} %collective-permute-done.1.refs_2_), channel_id=1, source_target_pairs={{0,64},{1,9},{8,72},{9,1},{16,80},{17,25},{24,88},{25,17},{32,96},... | collective-permute-start | bytes 1769480 | tf_op jit(solution)/shard_map/ppermute | solution.py:36
  60.5 12.2 %collective-permute-start.3 = (bf16[8,96,384]{2,1,0:T(8,128)(2,1)S(1)}, bf16[8,96,384]{2,1,0:T(8,128)(2,1)S(1)}, u32[]{:S(2)}, u32[]{:S(2)}) collective-permute-start(bf16[8,96,384]{2,1,0:T(8,128)(2,1)S(1)} %collective-permute-done.refs_1_), channel_id=1, source_target_pairs={{0,960},{1,57},{8,968},{9,17},{16,976},{17,9},{24,984},{25,33},{32... | collective-permute-start | bytes 1769480 | tf_op jit(solution)/shard_map/ppermute | solution.py:36
  66.8 12.2 %collective-permute-start.5 = (bf16[8,96,384]{2,1,0:T(8,128)(2,1)S(1)}, bf16[8,96,384]{2,1,0:T(8,128)(2,1)}, u32[]{:S(2)}, u32[]{:S(2)}) collective-permute-start(bf16[8,96,384]{2,1,0:T(8,128)(2,1)S(1)} %collective-permute-done.2.refs_3_), channel_id=1, source_target_pairs={{0,960},{1,57},{8,968},{9,17},{16,976},{17,9},{24,984},{25,33},{32... | collective-permute-start | bytes 1769480 | tf_op jit(solution)/shard_map/ppermute | solution.py:36
  72.7 11.0 %collective-permute-start.4 = (bf16[8,96,384]{2,1,0:T(8,128)(2,1)S(1)}, bf16[8,96,384]{2,1,0:T(8,128)(2,1)}, u32[]{:S(2)}, u32[]{:S(2)}) collective-permute-start(bf16[8,96,384]{2,1,0:T(8,128)(2,1)S(1)} %collective-permute-done.3.refs_4_), channel_id=1, source_target_pairs={{0,64},{1,9},{8,72},{9,1},{16,80},{17,25},{24,88},{25,17},{32,96},... | collective-permute-start | bytes 1769480 | tf_op jit(solution)/shard_map/ppermute | solution.py:36
  79.0 11.1 %collective-permute-start.6 = (bf16[8,96,384]{2,1,0:T(8,128)(2,1)}, bf16[8,96,384]{2,1,0:T(8,128)(2,1)S(1)}, u32[]{:S(2)}, u32[]{:S(2)}) collective-permute-start(bf16[8,96,384]{2,1,0:T(8,128)(2,1)} %collective-permute-done.5.refs_6_), channel_id=1, source_target_pairs={{0,64},{1,9},{8,72},{9,1},{16,80},{17,25},{24,88},{25,17},{32,96},... | collective-permute-start | bytes 1769480 | tf_op jit(solution)/shard_map/ppermute | solution.py:36
  91.8 7.9 %collective-permute-start.7 = (bf16[4,64,2048]{2,1,0:T(8,128)(2,1)S(1)}, bf16[4,64,2048]{2,1,0:T(8,128)(2,1)S(1)}, u32[]{:S(2)}, u32[]{:S(2)}) collective-permute-start(bf16[4,64,2048]{2,1,0:T(8,128)(2,1)S(1)} %shard_map.65), channel_id=1, source_target_pairs={{0,1},{1,0},{2,3},{3,2},{4,5},{5,4},{6,7},{7,6},{8,9},{9,8},{10,11... | collective-permute-start | bytes 3145736 | tf_op jit(solution)/shard_map/ppermute | solution.py:155
  99.1 20.2 %copy-start.2 = (f32[2048]{0:T(1024)S(1)}, f32[2048]{0:T(1024)}, u32[]{:S(2)}) copy-start(f32[2048]{0:T(1024)} %param.11) | copy-start | bytes 24580
  99.9 15.9 %collective-permute-start.10 = (bf16[64,2048]{1,0:T(8,128)(2,1)S(1)}, bf16[64,2048]{1,0:T(8,128)(2,1)S(1)}, u32[]{:S(2)}, u32[]{:S(2)}) collective-permute-start(bf16[64,2048]{1,0:T(8,128)(2,1)S(1)} %get-tuple-element.12), channel_id=1, source_target_pairs={{0,6},{2,4},{4,2},{6,0},{1,7},{3,5},{5,3},{7,1},{8,14},{10,12},{12... | collective-permute-start | bytes 786440 | tf_op jit(solution)/shard_map/ppermute | solution.py:161
  104.8 11.0 %collective-permute-start.8 = (bf16[64,2048]{1,0:T(8,128)(2,1)S(1)}, bf16[64,2048]{1,0:T(8,128)(2,1)S(1)}, u32[]{:S(2)}, u32[]{:S(2)}) collective-permute-start(bf16[64,2048]{1,0:T(8,128)(2,1)S(1)} %get-tuple-element.11), channel_id=1, source_target_pairs={{0,4},{2,6},{4,0},{6,2},{1,5},{3,7},{5,1},{7,3},{8,12},{10,14},{12... | collective-permute-start | bytes 786440 | tf_op jit(solution)/shard_map/ppermute | solution.py:161
  107.3 11.7 %collective-permute-start.9 = (bf16[64,2048]{1,0:T(8,128)(2,1)S(1)}, bf16[64,2048]{1,0:T(8,128)(2,1)S(1)}, u32[]{:S(2)}, u32[]{:S(2)}) collective-permute-start(bf16[64,2048]{1,0:T(8,128)(2,1)S(1)} %get-tuple-element.13), channel_id=1, source_target_pairs={{0,2},{2,0},{4,6},{6,4},{1,3},{3,1},{5,7},{7,5},{8,10},{10,8},{12,... | collective-permute-start | bytes 786440 | tf_op jit(solution)/shard_map/ppermute | solution.py:161

commit v4 on v3

--- a/solution.py
+++ b/solution.py
@@ -34,6 +34,13 @@
             pairs.append((here, (partner(z, kind) % 16 * 8 + y) * 2))
             pairs.append((here + 1, (z * 8 + partner(y, kind) % 8) * 2 + 1))
     return lax.ppermute(x, PLANE, pairs)
+
+
+def copies_kernel(w_gate, w_up, w_down, out):
+    for k in range(8):
+        out[k, 0:32] = w_gate[...]
+        out[k, 32:64] = w_up[...]
+        out[k, 64:96] = w_down[...]
 
 
 def most_kernel(ids, normed, *refs):
@@ -133,8 +140,13 @@
 
 
 def body(tokens, norm_gain, w_gate, w_up, w_down, post_gain):
-    own = jnp.concatenate([w_gate, w_up, w_down.T], axis=0)
-    own = jnp.broadcast_to(own[None], (8, *own.shape))
+    own = pl.pallas_call(
+        copies_kernel,
+        out_shape=jax.ShapeDtypeStruct((8, 96, 384), jnp.bfloat16),
+        in_specs=[VMEM] * 3,
+        out_specs=VMEM,
+        name="copies",
+    )(w_gate, w_up, w_down.T)
     block = lax.all_to_all(own, PLANE, 0, 0, tiled=True, axis_index_groups=first_groups())
     own_normed = rms_scale(tokens.astype(jnp.float32), norm_gain).astype(jnp.bfloat16)
     copies = jnp.broadcast_to(own_normed[None], (8, *own_normed.shape))

time: 121 us -> 121 us (level)
  Pallas kernels: 8.41 us -> 10.1 us
    pallas_call x0 -> x1, Pallas kernels: none -> 1.68 us  [body(): pl.pallas_call(copies_kernel, out_shape=jax.ShapeDtypeStruct((8, 96, 384)...]
where the time goes in v4:
time: 121 us; the launch traced here: 120 us
  starting transfers between devices  57.4 us (47%)
  waiting for transfers between devices  48 us (40%)
  Pallas kernels  10.1 us (8%)
  other arithmetic  2.87 us (2%)
  local copies, waits for them, and re-layouts  1.59 us (1%)
    ppermute x7, waiting for transfers between devices, exchange(): return lax.ppermute(x, PLANE, pairs)  22.4 us
    ppermute x7, starting transfers between devices, exchange(): return lax.ppermute(x, PLANE, pairs)  21.9 us
    all_to_all x1, starting transfers between devices, body(): lax.all_to_all(own, PLANE, 0, 0, tiled=True, axis_index_groups=first_grou...  16.2 us
    all_to_all x1, waiting for transfers between devices, body(): lax.all_to_all(own, PLANE, 0, 0, tiled=True, axis_index_groups=first_grou...  15.3 us
    ppermute x3, waiting for transfers between devices, body(): lax.ppermute(pair[k].astype(jnp.bfloat16), 'x', [(x, x ^ k) for x in rang...  9.75 us
    ppermute x3, starting transfers between devices, body(): lax.ppermute(pair[k].astype(jnp.bfloat16), 'x', [(x, x ^ k) for x in rang...  9.27 us
    ppermute x1, starting transfers between devices, body(): other = lax.ppermute(send, 'c', [(0, 1), (1, 0)])  5.65 us
    pallas_call x1, Pallas kernels, most_of(): pl.pallas_call(most_kernel, out_shape=(jax.ShapeDtypeStruct((2, 4, 2, 64,...  5.18 us
  transfers between devices with their start and end apart: 13, of which 10 were waited for; matrix products, arithmetic and copies ran while one was open for 2% of the time, Pallas kernels for 6%

profile of v4, /device:TPU:1, one launch (start us, length us, event | category | flops | bytes accessed | tf_op | source)
XLA Modules:
  0.0 120.2 jit_solution(17143364537867018274)
XLA Ops:
  0.0 0.0 copy-start
  0.0 0.0 copy-start.1
  0.0 1.7 %copies.1 = bf16[8,96,384]{2,1,0:T(8,128)(2,1)} custom-call(bf16[32,384]{1,0:T(8,128)(2,1)} %w_gate.1, bf16[32,384]{1,0:T(8,128)(2,1)} %w_up.1, bf16[32,384]{1,0:T(8,128)(2,1)} %bitcast.21), custom_call_target="tpu_custom_call" | custom-call | tf_op jit(solution)/shard_map/copies/pallas_call | solution.py:143
  1.7 16.2 %all-to-all-start.1 = ((bf16[8,96,384]{2,1,0:T(8,128)(2,1)}), bf16[8,96,384]{2,1,0:T(8,128)(2,1)S(1)}, u32[]{:S(2)}, u32[]{:S(2)}) async-start(bf16[8,96,384]{2,1,0:T(8,128)(2,1)} %copies.1), calls=%async_computation.1 | async-start | bytes 1179648 | tf_op jit(solution)/shard_map/all_to_all | solution.py:150
  17.9 1.1 fusion
  19.0 15.3 %all-to-all-done.1.refs_0_ = bf16[8,96,384]{2,1,0:T(8,128)(2,1)S(1)} async-done(((bf16[8,96,384]{2,1,0:T(8,128)(2,1)}), bf16[8,96,384]{2,1,0:T(8,128)(2,1)S(1)}, u32[]{:S(2)}, u32[]{:S(2)}) %all-to-all-start.1) | async-done | bytes 589856 | tf_op jit(solution)/shard_map/all_to_all | solution.py:150
  34.3 8.9 %collective-permute-start.1 = (bf16[8,96,384]{2,1,0:T(8,128)(2,1)S(1)}, bf16[8,96,384]{2,1,0:T(8,128)(2,1)S(1)}, u32[]{:S(2)}, u32[]{:S(2)}) collective-permute-start(bf16[8,96,384]{2,1,0:T(8,128)(2,1)S(1)} %all-to-all-done.1.refs_0_), channel_id=1, source_target_pairs={{0,960},{1,57},{8,968},{9,17},{16,976},{17,9},{24,984},{25,33},{32... | collective-permute-start | bytes 1769480 | tf_op jit(solution)/shard_map/ppermute | solution.py:36
  43.3 0.0 copy-done
  43.3 0.0 copy-done.1
  43.3 0.1 fusion.2
  43.5 1.6 %broadcast_in_dim.2 = bf16[8,64,2048]{2,1,0:T(8,128)(2,1)} broadcast(bf16[64,2048]{1,0:T(8,128)(2,1)S(1)} %fusion.2), dimensions={1,2} | broadcast | bytes 2359296 | tf_op jit(solution)/shard_map/broadcast_in_dim | solution.py:152
  45.0 4.4 %all-to-all-start = ((bf16[8,64,2048]{2,1,0:T(8,128)(2,1)}), bf16[8,64,2048]{2,1,0:T(8,128)(2,1)}, u32[]{:S(2)}, u32[]{:S(2)}) async-start(bf16[8,64,2048]{2,1,0:T(8,128)(2,1)} %broadcast_in_dim.2), calls=%async_computation | async-start | bytes 4194304 | tf_op jit(solution)/shard_map/all_to_all | solution.py:161
  49.4 1.9 %collective-permute-start = (bf16[8,96,384]{2,1,0:T(8,128)(2,1)S(1)}, bf16[8,96,384]{2,1,0:T(8,128)(2,1)S(1)}, u32[]{:S(2)}, u32[]{:S(2)}) collective-permute-start(bf16[8,96,384]{2,1,0:T(8,128)(2,1)S(1)} %all-to-all-done.1.refs_0_), channel_id=1, source_target_pairs={{0,64},{1,9},{8,72},{9,1},{16,80},{17,25},{24,88},{25,17},{32,96},... | collective-permute-start | bytes 1769480 | tf_op jit(solution)/shard_map/ppermute | solution.py:36
  51.4 0.0 collective-permute-done.1.refs_2_
  51.4 3.4 %collective-permute-start.2 = (bf16[8,96,384]{2,1,0:T(8,128)(2,1)S(1)}, bf16[8,96,384]{2,1,0:T(8,128)(2,1)S(1)}, u32[]{:S(2)}, u32[]{:S(2)}) collective-permute-start(bf16[8,96,384]{2,1,0:T(8,128)(2,1)S(1)} %collective-permute-done.1.refs_2_), channel_id=1, source_target_pairs={{0,64},{1,9},{8,72},{9,1},{16,80},{17,25},{24,88},{25,17},{32,96},... | collective-permute-start | bytes 1769480 | tf_op jit(solution)/shard_map/ppermute | solution.py:36
  54.7 5.7 %collective-permute-done.refs_1_ = bf16[8,96,384]{2,1,0:T(8,128)(2,1)S(1)} collective-permute-done((bf16[8,96,384]{2,1,0:T(8,128)(2,1)S(1)}, bf16[8,96,384]{2,1,0:T(8,128)(2,1)S(1)}, u32[]{:S(2)}, u32[]{:S(2)}) %collective-permute-start) | collective-permute-done | bytes 589856 | tf_op jit(solution)/shard_map/ppermute | solution.py:36
  60.5 1.9 %collective-permute-start.3 = (bf16[8,96,384]{2,1,0:T(8,128)(2,1)S(1)}, bf16[8,96,384]{2,1,0:T(8,128)(2,1)S(1)}, u32[]{:S(2)}, u32[]{:S(2)}) collective-permute-start(bf16[8,96,384]{2,1,0:T(8,128)(2,1)S(1)} %collective-permute-done.refs_1_), channel_id=1, source_target_pairs={{0,960},{1,57},{8,968},{9,17},{16,976},{17,9},{24,984},{25,33},{32... | collective-permute-start | bytes 1769480 | tf_op jit(solution)/shard_map/ppermute | solution.py:36
  62.4 4.4 %collective-permute-done.2.refs_3_ = bf16[8,96,384]{2,1,0:T(8,128)(2,1)S(1)} collective-permute-done((bf16[8,96,384]{2,1,0:T(8,128)(2,1)S(1)}, bf16[8,96,384]{2,1,0:T(8,128)(2,1)S(1)}, u32[]{:S(2)}, u32[]{:S(2)}) %collective-permute-start.2) | collective-permute-done | bytes 589856 | tf_op jit(solution)/shard_map/ppermute | solution.py:36
  66.8 1.9 %collective-permute-start.5 = (bf16[8,96,384]{2,1,0:T(8,128)(2,1)S(1)}, bf16[8,96,384]{2,1,0:T(8,128)(2,1)}, u32[]{:S(2)}, u32[]{:S(2)}) collective-permute-start(bf16[8,96,384]{2,1,0:T(8,128)(2,1)S(1)} %collective-permute-done.2.refs_3_), channel_id=1, source_target_pairs={{0,960},{1,57},{8,968},{9,17},{16,976},{17,9},{24,984},{25,33},{32... | collective-permute-start | bytes 1769480 | tf_op jit(solution)/shard_map/ppermute | solution.py:36
  68.7 4.0 %collective-permute-done.3.refs_4_ = bf16[8,96,384]{2,1,0:T(8,128)(2,1)S(1)} collective-permute-done((bf16[8,96,384]{2,1,0:T(8,128)(2,1)S(1)}, bf16[8,96,384]{2,1,0:T(8,128)(2,1)S(1)}, u32[]{:S(2)}, u32[]{:S(2)}) %collective-permute-start.3) | collective-permute-done | bytes 589856 | tf_op jit(solution)/shard_map/ppermute | solution.py:36
  72.7 1.9 %collective-permute-start.4 = (bf16[8,96,384]{2,1,0:T(8,128)(2,1)S(1)}, bf16[8,96,384]{2,1,0:T(8,128)(2,1)}, u32[]{:S(2)}, u32[]{:S(2)}) collective-permute-start(bf16[8,96,384]{2,1,0:T(8,128)(2,1)S(1)} %collective-permute-done.3.refs_4_), channel_id=1, source_target_pairs={{0,64},{1,9},{8,72},{9,1},{16,80},{17,25},{24,88},{25,17},{32,96},... | collective-permute-start | bytes 1769480 | tf_op jit(solution)/shard_map/ppermute | solution.py:36
  74.6 4.4 %collective-permute-done.5.refs_6_ = bf16[8,96,384]{2,1,0:T(8,128)(2,1)} collective-permute-done((bf16[8,96,384]{2,1,0:T(8,128)(2,1)S(1)}, bf16[8,96,384]{2,1,0:T(8,128)(2,1)}, u32[]{:S(2)}, u32[]{:S(2)}) %collective-permute-start.5) | collective-permute-done | bytes 589856 | tf_op jit(solution)/shard_map/ppermute | solution.py:36
  79.0 1.9 %collective-permute-start.6 = (bf16[8,96,384]{2,1,0:T(8,128)(2,1)}, bf16[8,96,384]{2,1,0:T(8,128)(2,1)S(1)}, u32[]{:S(2)}, u32[]{:S(2)}) collective-permute-start(bf16[8,96,384]{2,1,0:T(8,128)(2,1)} %collective-permute-done.5.refs_6_), channel_id=1, source_target_pairs={{0,64},{1,9},{8,72},{9,1},{16,80},{17,25},{24,88},{25,17},{32,96},... | collective-permute-start | bytes 1769480 | tf_op jit(solution)/shard_map/ppermute | solution.py:36
  80.9 0.1 add_add_fusion.1.ids
  81.0 0.0 all-to-all-done.normed
  81.0 2.7 %collective-permute-done.4.refs_5_ = bf16[8,96,384]{2,1,0:T(8,128)(2,1)} collective-permute-done((bf16[8,96,384]{2,1,0:T(8,128)(2,1)S(1)}, bf16[8,96,384]{2,1,0:T(8,128)(2,1)}, u32[]{:S(2)}, u32[]{:S(2)}) %collective-permute-start.4) | collective-permute-done | bytes 589856 | tf_op jit(solution)/shard_map/ppermute | solution.py:36
  83.7 5.2 %most.1 = (f32[2,4,2,64,384]{4,3,2,1,0:T(8,128)S(1)}, bf16[4,2,64,256]{3,2,1,0:T(8,128)(2,1)S(1)}, bf16[8,8,32,384]{3,2,1,0:T(8,128)(2,1)S(1)}) custom-call(s32[4]{0:T(128)S(1)} %add_add_fusion.1.ids, bf16[8,64,2048]{2,1,0:T(8,128)(2,1)} %all-to-all-done.normed, bf16[8,96,384]{2,1,0:T(8,128)(2,1)S(1)} %all-to-all-done.1.refs_0_, ...), custom_call_target="tpu_custom_call" | custom-call | tf_op jit(solution)/shard_map/most/pallas_call | solution.py:116
  88.9 1.2 %collective-permute-done.6.blk = bf16[8,96,384]{2,1,0:T(8,128)(2,1)S(1)} collective-permute-done((bf16[8,96,384]{2,1,0:T(8,128)(2,1)}, bf16[8,96,384]{2,1,0:T(8,128)(2,1)S(1)}, u32[]{:S(2)}, u32[]{:S(2)}) %collective-permute-start.6) | collective-permute-done | bytes 589856 | tf_op jit(solution)/shard_map/ppermute | solution.py:36
  90.1 1.6 %shard_map.65 = bf16[4,64,2048]{2,1,0:T(8,128)(2,1)S(1)} custom-call(s32[4]{0:T(128)S(1)} %add_add_fusion.1.ids, f32[2,4,2,64,384]{4,3,2,1,0:T(8,128)S(1)} %get-tuple-element.8.gate_up, bf16[4,2,64,256]{3,2,1,0:T(8,128)(2,1)S(1)} %get-tuple-element.9.x_last, bf16[8,8,32,384]{3,2,1,0:T(8,128)(2,1)S(1)} %get-tuple-element.10.most_down, ...), custom_call_target="tpu_custom_call" | custom-call | tf_op jit(solution)/shard_map/pallas_call | solution.py:132
  91.8 5.6 %collective-permute-start.7 = (bf16[4,64,2048]{2,1,0:T(8,128)(2,1)S(1)}, bf16[4,64,2048]{2,1,0:T(8,128)(2,1)S(1)}, u32[]{:S(2)}, u32[]{:S(2)}) collective-permute-start(bf16[4,64,2048]{2,1,0:T(8,128)(2,1)S(1)} %shard_map.65), channel_id=1, source_target_pairs={{0,1},{1,0},{2,3},{3,2},{4,5},{5,4},{6,7},{7,6},{8,9},{9,8},{10,11... | collective-permute-start | bytes 3145736 | tf_op jit(solution)/shard_map/ppermute | solution.py:167
  97.4 0.1 add_add_fusion.ids
  97.5 1.6 %shard_map.64 = bf16[4,64,2048]{2,1,0:T(8,128)(2,1)S(1)} custom-call(s32[4]{0:T(128)S(1)} %add_add_fusion.ids, f32[2,4,2,64,384]{4,3,2,1,0:T(8,128)S(1)} %get-tuple-element.8.gate_up, bf16[4,2,64,256]{3,2,1,0:T(8,128)(2,1)S(1)} %get-tuple-element.9.x_last, bf16[8,8,32,384]{3,2,1,0:T(8,128)(2,1)S(1)} %get-tuple-element.10.most_down, ...), custom_call_target="tpu_custom_call" | custom-call | tf_op jit(solution)/shard_map/pallas_call | solution.py:132
  99.1 0.0 copy-start.2
  99.1 0.5 collective-permute-done.7
  99.7 0.3 fusion.5
  99.9 4.9 %collective-permute-start.10 = (bf16[64,2048]{1,0:T(8,128)(2,1)S(1)}, bf16[64,2048]{1,0:T(8,128)(2,1)S(1)}, u32[]{:S(2)}, u32[]{:S(2)}) collective-permute-start(bf16[64,2048]{1,0:T(8,128)(2,1)S(1)} %get-tuple-element.12), channel_id=1, source_target_pairs={{0,6},{2,4},{4,2},{6,0},{1,7},{3,5},{5,3},{7,1},{8,14},{10,12},{12... | collective-permute-start | bytes 786440 | tf_op jit(solution)/shard_map/ppermute | solution.py:173
  104.8 2.5 %collective-permute-start.8 = (bf16[64,2048]{1,0:T(8,128)(2,1)S(1)}, bf16[64,2048]{1,0:T(8,128)(2,1)S(1)}, u32[]{:S(2)}, u32[]{:S(2)}) collective-permute-start(bf16[64,2048]{1,0:T(8,128)(2,1)S(1)} %get-tuple-element.11), channel_id=1, source_target_pairs={{0,4},{2,6},{4,0},{6,2},{1,5},{3,7},{5,1},{7,3},{8,12},{10,14},{12... | collective-permute-start | bytes 786440 | tf_op jit(solution)/shard_map/ppermute | solution.py:173
  107.3 1.9 %collective-permute-start.9 = (bf16[64,2048]{1,0:T(8,128)(2,1)S(1)}, bf16[64,2048]{1,0:T(8,128)(2,1)S(1)}, u32[]{:S(2)}, u32[]{:S(2)}) collective-permute-start(bf16[64,2048]{1,0:T(8,128)(2,1)S(1)} %get-tuple-element.13), channel_id=1, source_target_pairs={{0,2},{2,0},{4,6},{6,4},{1,3},{3,1},{5,7},{7,5},{8,10},{10,8},{12,... | collective-permute-start | bytes 786440 | tf_op jit(solution)/shard_map/ppermute | solution.py:173
  109.2 6.6 %collective-permute-done.10 = bf16[64,2048]{1,0:T(8,128)(2,1)S(1)} collective-permute-done((bf16[64,2048]{1,0:T(8,128)(2,1)S(1)}, bf16[64,2048]{1,0:T(8,128)(2,1)S(1)}, u32[]{:S(2)}, u32[]{:S(2)}) %collective-permute-start.10) | collective-permute-done | bytes 262176 | tf_op jit(solution)/shard_map/ppermute | solution.py:173
  115.8 0.0 collective-permute-done.8
  115.8 3.2 %collective-permute-done.9 = bf16[64,2048]{1,0:T(8,128)(2,1)S(1)} collective-permute-done((bf16[64,2048]{1,0:T(8,128)(2,1)S(1)}, bf16[64,2048]{1,0:T(8,128)(2,1)S(1)}, u32[]{:S(2)}, u32[]{:S(2)}) %collective-permute-start.9) | collective-permute-done | bytes 262176 | tf_op jit(solution)/shard_map/ppermute | solution.py:173
  119.0 0.3 multiply_reduce_fusion
  119.3 0.0 copy-done.2
  119.3 0.9 multiply_convert_fusion
  (2 shorter events, 0.0 us)
Async XLA Ops:
  0.0 43.3 %copy-start = (bf16[64,2048]{1,0:T(8,128)(2,1)S(1)}, bf16[64,2048]{1,0:T(8,128)(2,1)}, u32[]{:S(2)}) copy-start(bf16[64,2048]{1,0:T(8,128)(2,1)} %param.6) | copy-start | bytes 786436
  0.0 43.3 %copy-start.1 = (f32[2048]{0:T(1024)S(1)}, f32[2048]{0:T(1024)}, u32[]{:S(2)}) copy-start(f32[2048]{0:T(1024)} %param.7) | copy-start | bytes 24580
  1.7 32.7 %all-to-all-start.1 = ((bf16[8,96,384]{2,1,0:T(8,128)(2,1)}), bf16[8,96,384]{2,1,0:T(8,128)(2,1)S(1)}, u32[]{:S(2)}, u32[]{:S(2)}) async-start(bf16[8,96,384]{2,1,0:T(8,128)(2,1)} %copies.1), calls=%async_computation.1 | async-start | bytes 1179648 | tf_op jit(solution)/shard_map/all_to_all | solution.py:150
  34.3 17.0 %collective-permute-start.1 = (bf16[8,96,384]{2,1,0:T(8,128)(2,1)S(1)}, bf16[8,96,384]{2,1,0:T(8,128)(2,1)S(1)}, u32[]{:S(2)}, u32[]{:S(2)}) collective-permute-start(bf16[8,96,384]{2,1,0:T(8,128)(2,1)S(1)} %all-to-all-done.1.refs_0_), channel_id=1, source_target_pairs={{0,960},{1,57},{8,968},{9,17},{16,976},{17,9},{24,984},{25,33},{32... | collective-permute-start | bytes 1769480 | tf_op jit(solution)/shard_map/ppermute | solution.py:36
  45.0 36.0 %all-to-all-start = ((bf16[8,64,2048]{2,1,0:T(8,128)(2,1)}), bf16[8,64,2048]{2,1,0:T(8,128)(2,1)}, u32[]{:S(2)}, u32[]{:S(2)}) async-start(bf16[8,64,2048]{2,1,0:T(8,128)(2,1)} %broadcast_in_dim.2), calls=%async_computation | async-start | bytes 4194304 | tf_op jit(solution)/shard_map/all_to_all | solution.py:161
  49.4 11.0 %collective-permute-start = (bf16[8,96,384]{2,1,0:T(8,128)(2,1)S(1)}, bf16[8,96,384]{2,1,0:T(8,128)(2,1)S(1)}, u32[]{:S(2)}, u32[]{:S(2)}) collective-permute-start(bf16[8,96,384]{2,1,0:T(8,128)(2,1)S(1)} %all-to-all-done.1.refs_0_), channel_id=1, source_target_pairs={{0,64},{1,9},{8,72},{9,1},{16,80},{17,25},{24,88},{25,17},{32,96},... | collective-permute-start | bytes 1769480 | tf_op jit(solution)/shard_map/ppermute | solution.py:36
  51.4 15.4 %collective-permute-start.2 = (bf16[8,96,384]{2,1,0:T(8,128)(2,1)S(1)}, bf16[8,96,384]{2,1,0:T(8,128)(2,1)S(1)}, u32[]{:S(2)}, u32[]{:S(2)}) collective-permute-start(bf16[8,96,384]{2,1,0:T(8,128)(2,1)S(1)} %collective-permute-done.1.refs_2_), channel_id=1, source_target_pairs={{0,64},{1,9},{8,72},{9,1},{16,80},{17,25},{24,88},{25,17},{32,96},... | collective-permute-start | bytes 1769480 | tf_op jit(solution)/shard_map/ppermute | solution.py:36
  60.5 12.2 %collective-permute-start.3 = (bf16[8,96,384]{2,1,0:T(8,128)(2,1)S(1)}, bf16[8,96,384]{2,1,0:T(8,128)(2,1)S(1)}, u32[]{:S(2)}, u32[]{:S(2)}) collective-permute-start(bf16[8,96,384]{2,1,0:T(8,128)(2,1)S(1)} %collective-permute-done.refs_1_), channel_id=1, source_target_pairs={{0,960},{1,57},{8,968},{9,17},{16,976},{17,9},{24,984},{25,33},{32... | collective-permute-start | bytes 1769480 | tf_op jit(solution)/shard_map/ppermute | solution.py:36
  66.8 12.2 %collective-permute-start.5 = (bf16[8,96,384]{2,1,0:T(8,128)(2,1)S(1)}, bf16[8,96,384]{2,1,0:T(8,128)(2,1)}, u32[]{:S(2)}, u32[]{:S(2)}) collective-permute-start(bf16[8,96,384]{2,1,0:T(8,128)(2,1)S(1)} %collective-permute-done.2.refs_3_), channel_id=1, source_target_pairs={{0,960},{1,57},{8,968},{9,17},{16,976},{17,9},{24,984},{25,33},{32... | collective-permute-start | bytes 1769480 | tf_op jit(solution)/shard_map/ppermute | solution.py:36
  72.7 11.0 %collective-permute-start.4 = (bf16[8,96,384]{2,1,0:T(8,128)(2,1)S(1)}, bf16[8,96,384]{2,1,0:T(8,128)(2,1)}, u32[]{:S(2)}, u32[]{:S(2)}) collective-permute-start(bf16[8,96,384]{2,1,0:T(8,128)(2,1)S(1)} %collective-permute-done.3.refs_4_), channel_id=1, source_target_pairs={{0,64},{1,9},{8,72},{9,1},{16,80},{17,25},{24,88},{25,17},{32,96},... | collective-permute-start | bytes 1769480 | tf_op jit(solution)/shard_map/ppermute | solution.py:36
  79.0 11.1 %collective-permute-start.6 = (bf16[8,96,384]{2,1,0:T(8,128)(2,1)}, bf16[8,96,384]{2,1,0:T(8,128)(2,1)S(1)}, u32[]{:S(2)}, u32[]{:S(2)}) collective-permute-start(bf16[8,96,384]{2,1,0:T(8,128)(2,1)} %collective-permute-done.5.refs_6_), channel_id=1, source_target_pairs={{0,64},{1,9},{8,72},{9,1},{16,80},{17,25},{24,88},{25,17},{32,96},... | collective-permute-start | bytes 1769480 | tf_op jit(solution)/shard_map/ppermute | solution.py:36
  91.8 7.9 %collective-permute-start.7 = (bf16[4,64,2048]{2,1,0:T(8,128)(2,1)S(1)}, bf16[4,64,2048]{2,1,0:T(8,128)(2,1)S(1)}, u32[]{:S(2)}, u32[]{:S(2)}) collective-permute-start(bf16[4,64,2048]{2,1,0:T(8,128)(2,1)S(1)} %shard_map.65), channel_id=1, source_target_pairs={{0,1},{1,0},{2,3},{3,2},{4,5},{5,4},{6,7},{7,6},{8,9},{9,8},{10,11... | collective-permute-start | bytes 3145736 | tf_op jit(solution)/shard_map/ppermute | solution.py:167
  99.1 20.2 %copy-start.2 = (f32[2048]{0:T(1024)S(1)}, f32[2048]{0:T(1024)}, u32[]{:S(2)}) copy-start(f32[2048]{0:T(1024)} %param.11) | copy-start | bytes 24580
  99.9 15.9 %collective-permute-start.10 = (bf16[64,2048]{1,0:T(8,128)(2,1)S(1)}, bf16[64,2048]{1,0:T(8,128)(2,1)S(1)}, u32[]{:S(2)}, u32[]{:S(2)}) collective-permute-start(bf16[64,2048]{1,0:T(8,128)(2,1)S(1)} %get-tuple-element.12), channel_id=1, source_target_pairs={{0,6},{2,4},{4,2},{6,0},{1,7},{3,5},{5,3},{7,1},{8,14},{10,12},{12... | collective-permute-start | bytes 786440 | tf_op jit(solution)/shard_map/ppermute | solution.py:173
  104.8 11.0 %collective-permute-start.8 = (bf16[64,2048]{1,0:T(8,128)(2,1)S(1)}, bf16[64,2048]{1,0:T(8,128)(2,1)S(1)}, u32[]{:S(2)}, u32[]{:S(2)}) collective-permute-start(bf16[64,2048]{1,0:T(8,128)(2,1)S(1)} %get-tuple-element.11), channel_id=1, source_target_pairs={{0,4},{2,6},{4,0},{6,2},{1,5},{3,7},{5,1},{7,3},{8,12},{10,14},{12... | collective-permute-start | bytes 786440 | tf_op jit(solution)/shard_map/ppermute | solution.py:173
  107.3 11.7 %collective-permute-start.9 = (bf16[64,2048]{1,0:T(8,128)(2,1)S(1)}, bf16[64,2048]{1,0:T(8,128)(2,1)S(1)}, u32[]{:S(2)}, u32[]{:S(2)}) collective-permute-start(bf16[64,2048]{1,0:T(8,128)(2,1)S(1)} %get-tuple-element.13), channel_id=1, source_target_pairs={{0,2},{2,0},{4,6},{6,4},{1,3},{3,1},{5,7},{7,5},{8,10},{10,8},{12,... | collective-permute-start | bytes 786440 | tf_op jit(solution)/shard_map/ppermute | solution.py:173

commit v5 on v3

--- a/solution.py
+++ b/solution.py
@@ -72,7 +72,7 @@
     x_last[...] = picked.astype(jnp.bfloat16).reshape(4, 2, 64, 256)
 
 
-def last_kernel(ids, gate_up, x_last, most_down, blk, out, down):
+def last_kernel(ids, gate_up, x_last, most_down, blk, out, out_own, down):
     base, core, which = ids[0], ids[1], ids[2]
     last = (base + 4) & 7
     down[...] = most_down[...]
@@ -97,7 +97,15 @@
     part = lax.dot_general(hidden, down[...].reshape(2048, 384), nt, preferred_element_type=jnp.float32)
     part = part.astype(jnp.bfloat16)
     for k in range(4):
-        out[ids[3] ^ k] = part[64 * k : 64 * k + 64]
+        to = ids[3] ^ k
+
+        @pl.when(to == 0)
+        def _():
+            out_own[...] = part[64 * k : 64 * k + 64]
+
+        @pl.when(to != 0)
+        def _():
+            out[to - 1] = part[64 * k : 64 * k + 64]
 
 
 VMEM = pl.BlockSpec(memory_space=pltpu.VMEM)
@@ -124,9 +132,9 @@
 def partial_of(ids, most, block):
     return pl.pallas_call(
         last_kernel,
-        out_shape=jax.ShapeDtypeStruct((4, 64, 2048), jnp.bfloat16),
+        out_shape=(jax.ShapeDtypeStruct((3, 64, 2048), jnp.bfloat16), jax.ShapeDtypeStruct((64, 2048), jnp.bfloat16)),
         in_specs=[SMEM] + [VMEM] * 4,
-        out_specs=VMEM,
+        out_specs=(VMEM, VMEM),
         scratch_shapes=[pltpu.VMEM(WHOLE, jnp.bfloat16)],
         compiler_params=pltpu.CompilerParams(vmem_limit_bytes=16 * 1024 * 1024),
     )(ids, *most, block)
@@ -151,14 +159,15 @@
     base = jnp.where(core == 0, lax.axis_index("zl"), lax.axis_index("y"))
     ids = jnp.stack([base, core, 1 - core, col]).astype(jnp.int32)
     most = most_of(ids, normed, blocks)
-    send = partial_of(ids, most, final)
+    send, send_own = partial_of(ids, most, final)
     other = lax.ppermute(send, "c", [(0, 1), (1, 0)])
+    other_own = lax.ppermute(send_own, "c", [(0, 1), (1, 0)])
     ids = jnp.stack([base, core, core, col]).astype(jnp.int32)
-    keep = partial_of(ids, most, final)
-    pair = [keep[k].astype(jnp.float32) + other[k].astype(jnp.float32) for k in range(4)]
-    summed = pair[0]
+    keep, keep_own = partial_of(ids, most, final)
+    pair = [keep[k].astype(jnp.float32) + other[k].astype(jnp.float32) for k in range(3)]
+    summed = keep_own.astype(jnp.float32) + other_own.astype(jnp.float32)
     for k in (2, 1, 3):
-        got = lax.ppermute(pair[k].astype(jnp.bfloat16), "x", [(x, x ^ k) for x in range(4)])
+        got = lax.ppermute(pair[k - 1].astype(jnp.bfloat16), "x", [(x, x ^ k) for x in range(4)])
         summed = summed + got.astype(jnp.float32)
     return rms_scale(summed, post_gain).astype(jnp.bfloat16)
 

time: 121 us -> 123 us (1.017)
  starting transfers between devices: 57.4 us -> 59.9 us
    ppermute x3 -> x4, starting transfers between devices: 9.27 us -> 11.8 us  [the longest x3 9.86 us: body(): lax.ppermute(pair[k - 1].astype(jnp.bfloat16), 'x', [(x, x ^ k) for x in...]
    ppermute x3 -> x4, waiting for transfers between devices: 9.75 us -> 9.56 us  [the longest x3 9.55 us: body(): lax.ppermute(pair[k - 1].astype(jnp.bfloat16), 'x', [(x, x ^ k) for x in...]
  transfers between devices with their start and end apart: 13 -> 14, of which waited for: 10 -> 8; matrix products, arithmetic and copies ran while one was open for 2% -> 2% of each run, Pallas kernels for 6% -> 6%
where the time goes in v5:
time: 123 us; the launch traced here: 122 us
  starting transfers between devices  59.9 us (49%)
  waiting for transfers between devices  48.2 us (39%)
  Pallas kernels  8.67 us (7%)
  other arithmetic  2.67 us (2%)
  local copies, waits for them, and re-layouts  2.47 us (2%)
    ppermute x7, waiting for transfers between devices, exchange(): return lax.ppermute(x, PLANE, pairs)  22.4 us
    ppermute x7, starting transfers between devices, exchange(): return lax.ppermute(x, PLANE, pairs)  21.9 us
    all_to_all x1, waiting for transfers between devices, body(): lax.all_to_all(own, PLANE, 0, 0, tiled=True, axis_index_groups=first_grou...  16.3 us
    all_to_all x1, starting transfers between devices, body(): lax.all_to_all(own, PLANE, 0, 0, tiled=True, axis_index_groups=first_grou...  16.2 us
    ppermute x3, starting transfers between devices, body(): lax.ppermute(pair[k - 1].astype(jnp.bfloat16), 'x', [(x, x ^ k) for x in...  9.86 us
    ppermute x3, waiting for transfers between devices, body(): lax.ppermute(pair[k - 1].astype(jnp.bfloat16), 'x', [(x, x ^ k) for x in...  9.55 us
    ppermute x1, starting transfers between devices, body(): other = lax.ppermute(send, 'c', [(0, 1), (1, 0)])  5.65 us
    pallas_call x1, Pallas kernels, most_of(): pl.pallas_call(most_kernel, out_shape=(jax.ShapeDtypeStruct((2, 4, 2, 64,...  5.18 us
  transfers between devices with their start and end apart: 14, of which 8 were waited for; matrix products, arithmetic and copies ran while one was open for 2% of the time, Pallas kernels for 6%

profile of v5, /device:TPU:1, one launch (start us, length us, event | category | flops | bytes accessed | tf_op | source)
XLA Modules:
  0.0 122.2 jit_solution(14836994897328237803)
XLA Ops:
  0.0 0.0 copy-start
  0.0 0.0 copy-start.1
  0.0 0.8 pad_maximum_fusion
  0.8 0.9 broadcast_in_dim.5
  1.7 16.2 %all-to-all-start.1 = ((bf16[8,96,384]{2,1,0:T(8,128)(2,1)}), bf16[8,96,384]{2,1,0:T(8,128)(2,1)S(1)}, u32[]{:S(2)}, u32[]{:S(2)}) async-start(bf16[8,96,384]{2,1,0:T(8,128)(2,1)} %broadcast_in_dim.5), calls=%async_computation.1 | async-start | bytes 1179648 | tf_op jit(solution)/shard_map/all_to_all | solution.py:146
  18.0 0.0 copy-done
  18.0 0.2 fusion
  18.1 16.3 %all-to-all-done.1.refs_0_ = bf16[8,96,384]{2,1,0:T(8,128)(2,1)S(1)} async-done(((bf16[8,96,384]{2,1,0:T(8,128)(2,1)}), bf16[8,96,384]{2,1,0:T(8,128)(2,1)S(1)}, u32[]{:S(2)}, u32[]{:S(2)}) %all-to-all-start.1) | async-done | bytes 589856 | tf_op jit(solution)/shard_map/all_to_all | solution.py:146
  34.4 8.9 %collective-permute-start.1 = (bf16[8,96,384]{2,1,0:T(8,128)(2,1)S(1)}, bf16[8,96,384]{2,1,0:T(8,128)(2,1)S(1)}, u32[]{:S(2)}, u32[]{:S(2)}) collective-permute-start(bf16[8,96,384]{2,1,0:T(8,128)(2,1)S(1)} %all-to-all-done.1.refs_0_), channel_id=1, source_target_pairs={{0,960},{1,57},{8,968},{9,17},{16,976},{17,9},{24,984},{25,33},{32... | collective-permute-start | bytes 1769480 | tf_op jit(solution)/shard_map/ppermute | solution.py:36
  43.3 0.0 copy-done.1
  43.3 0.1 fusion.2
  43.5 1.6 %broadcast_in_dim.4 = bf16[8,64,2048]{2,1,0:T(8,128)(2,1)} broadcast(bf16[64,2048]{1,0:T(8,128)(2,1)S(1)} %fusion.2), dimensions={1,2} | broadcast | bytes 2359296 | tf_op jit(solution)/shard_map/broadcast_in_dim | solution.py:148
  45.0 4.4 %all-to-all-start = ((bf16[8,64,2048]{2,1,0:T(8,128)(2,1)}), bf16[8,64,2048]{2,1,0:T(8,128)(2,1)}, u32[]{:S(2)}, u32[]{:S(2)}) async-start(bf16[8,64,2048]{2,1,0:T(8,128)(2,1)} %broadcast_in_dim.4), calls=%async_computation | async-start | bytes 4194304 | tf_op jit(solution)/shard_map/all_to_all | solution.py:157
  49.4 1.9 %collective-permute-start = (bf16[8,96,384]{2,1,0:T(8,128)(2,1)S(1)}, bf16[8,96,384]{2,1,0:T(8,128)(2,1)S(1)}, u32[]{:S(2)}, u32[]{:S(2)}) collective-permute-start(bf16[8,96,384]{2,1,0:T(8,128)(2,1)S(1)} %all-to-all-done.1.refs_0_), channel_id=1, source_target_pairs={{0,64},{1,9},{8,72},{9,1},{16,80},{17,25},{24,88},{25,17},{32,96},... | collective-permute-start | bytes 1769480 | tf_op jit(solution)/shard_map/ppermute | solution.py:36
  51.4 0.0 collective-permute-done.1.refs_2_
  51.4 3.4 %collective-permute-start.2 = (bf16[8,96,384]{2,1,0:T(8,128)(2,1)S(1)}, bf16[8,96,384]{2,1,0:T(8,128)(2,1)S(1)}, u32[]{:S(2)}, u32[]{:S(2)}) collective-permute-start(bf16[8,96,384]{2,1,0:T(8,128)(2,1)S(1)} %collective-permute-done.1.refs_2_), channel_id=1, source_target_pairs={{0,64},{1,9},{8,72},{9,1},{16,80},{17,25},{24,88},{25,17},{32,96},... | collective-permute-start | bytes 1769480 | tf_op jit(solution)/shard_map/ppermute | solution.py:36
  54.7 5.7 %collective-permute-done.refs_1_ = bf16[8,96,384]{2,1,0:T(8,128)(2,1)S(1)} collective-permute-done((bf16[8,96,384]{2,1,0:T(8,128)(2,1)S(1)}, bf16[8,96,384]{2,1,0:T(8,128)(2,1)S(1)}, u32[]{:S(2)}, u32[]{:S(2)}) %collective-permute-start) | collective-permute-done | bytes 589856 | tf_op jit(solution)/shard_map/ppermute | solution.py:36
  60.5 1.9 %collective-permute-start.3 = (bf16[8,96,384]{2,1,0:T(8,128)(2,1)S(1)}, bf16[8,96,384]{2,1,0:T(8,128)(2,1)S(1)}, u32[]{:S(2)}, u32[]{:S(2)}) collective-permute-start(bf16[8,96,384]{2,1,0:T(8,128)(2,1)S(1)} %collective-permute-done.refs_1_), channel_id=1, source_target_pairs={{0,960},{1,57},{8,968},{9,17},{16,976},{17,9},{24,984},{25,33},{32... | collective-permute-start | bytes 1769480 | tf_op jit(solution)/shard_map/ppermute | solution.py:36
  62.4 4.4 %collective-permute-done.2.refs_3_ = bf16[8,96,384]{2,1,0:T(8,128)(2,1)S(1)} collective-permute-done((bf16[8,96,384]{2,1,0:T(8,128)(2,1)S(1)}, bf16[8,96,384]{2,1,0:T(8,128)(2,1)S(1)}, u32[]{:S(2)}, u32[]{:S(2)}) %collective-permute-start.2) | collective-permute-done | bytes 589856 | tf_op jit(solution)/shard_map/ppermute | solution.py:36
  66.8 1.9 %collective-permute-start.5 = (bf16[8,96,384]{2,1,0:T(8,128)(2,1)S(1)}, bf16[8,96,384]{2,1,0:T(8,128)(2,1)}, u32[]{:S(2)}, u32[]{:S(2)}) collective-permute-start(bf16[8,96,384]{2,1,0:T(8,128)(2,1)S(1)} %collective-permute-done.2.refs_3_), channel_id=1, source_target_pairs={{0,960},{1,57},{8,968},{9,17},{16,976},{17,9},{24,984},{25,33},{32... | collective-permute-start | bytes 1769480 | tf_op jit(solution)/shard_map/ppermute | solution.py:36
  68.7 4.0 %collective-permute-done.3.refs_4_ = bf16[8,96,384]{2,1,0:T(8,128)(2,1)S(1)} collective-permute-done((bf16[8,96,384]{2,1,0:T(8,128)(2,1)S(1)}, bf16[8,96,384]{2,1,0:T(8,128)(2,1)S(1)}, u32[]{:S(2)}, u32[]{:S(2)}) %collective-permute-start.3) | collective-permute-done | bytes 589856 | tf_op jit(solution)/shard_map/ppermute | solution.py:36
  72.7 1.9 %collective-permute-start.4 = (bf16[8,96,384]{2,1,0:T(8,128)(2,1)S(1)}, bf16[8,96,384]{2,1,0:T(8,128)(2,1)}, u32[]{:S(2)}, u32[]{:S(2)}) collective-permute-start(bf16[8,96,384]{2,1,0:T(8,128)(2,1)S(1)} %collective-permute-done.3.refs_4_), channel_id=1, source_target_pairs={{0,64},{1,9},{8,72},{9,1},{16,80},{17,25},{24,88},{25,17},{32,96},... | collective-permute-start | bytes 1769480 | tf_op jit(solution)/shard_map/ppermute | solution.py:36
  74.6 4.4 %collective-permute-done.5.refs_6_ = bf16[8,96,384]{2,1,0:T(8,128)(2,1)} collective-permute-done((bf16[8,96,384]{2,1,0:T(8,128)(2,1)S(1)}, bf16[8,96,384]{2,1,0:T(8,128)(2,1)}, u32[]{:S(2)}, u32[]{:S(2)}) %collective-permute-start.5) | collective-permute-done | bytes 589856 | tf_op jit(solution)/shard_map/ppermute | solution.py:36
  79.0 1.9 %collective-permute-start.6 = (bf16[8,96,384]{2,1,0:T(8,128)(2,1)}, bf16[8,96,384]{2,1,0:T(8,128)(2,1)S(1)}, u32[]{:S(2)}, u32[]{:S(2)}) collective-permute-start(bf16[8,96,384]{2,1,0:T(8,128)(2,1)} %collective-permute-done.5.refs_6_), channel_id=1, source_target_pairs={{0,64},{1,9},{8,72},{9,1},{16,80},{17,25},{24,88},{25,17},{32,96},... | collective-permute-start | bytes 1769480 | tf_op jit(solution)/shard_map/ppermute | solution.py:36
  80.9 0.1 add_add_fusion
  81.0 0.0 all-to-all-done.normed
  81.0 2.7 %collective-permute-done.4.refs_5_ = bf16[8,96,384]{2,1,0:T(8,128)(2,1)} collective-permute-done((bf16[8,96,384]{2,1,0:T(8,128)(2,1)S(1)}, bf16[8,96,384]{2,1,0:T(8,128)(2,1)}, u32[]{:S(2)}, u32[]{:S(2)}) %collective-permute-start.4) | collective-permute-done | bytes 589856 | tf_op jit(solution)/shard_map/ppermute | solution.py:36
  83.7 5.2 %most.1 = (f32[2,4,2,64,384]{4,3,2,1,0:T(8,128)S(1)}, bf16[4,2,64,256]{3,2,1,0:T(8,128)(2,1)S(1)}, bf16[8,8,32,384]{3,2,1,0:T(8,128)(2,1)S(1)}) custom-call(s32[4]{0:T(128)S(1)} %get-tuple-element.23.ids, bf16[8,64,2048]{2,1,0:T(8,128)(2,1)} %all-to-all-done.normed, bf16[8,96,384]{2,1,0:T(8,128)(2,1)S(1)} %all-to-all-done.1.refs_0_, ...), custom_call_target="tpu_custom_call" | custom-call | tf_op jit(solution)/shard_map/most/pallas_call | solution.py:117
  88.9 1.2 %collective-permute-done.6.blk = bf16[8,96,384]{2,1,0:T(8,128)(2,1)S(1)} collective-permute-done((bf16[8,96,384]{2,1,0:T(8,128)(2,1)}, bf16[8,96,384]{2,1,0:T(8,128)(2,1)S(1)}, u32[]{:S(2)}, u32[]{:S(2)}) %collective-permute-start.6) | collective-permute-done | bytes 589856 | tf_op jit(solution)/shard_map/ppermute | solution.py:36
  90.1 1.7 %shard_map.65 = (bf16[3,64,2048]{2,1,0:T(8,128)(2,1)S(1)}, bf16[64,2048]{1,0:T(8,128)(2,1)S(1)}) custom-call(s32[4]{0:T(128)S(1)} %get-tuple-element.23.ids, f32[2,4,2,64,384]{4,3,2,1,0:T(8,128)S(1)} %get-tuple-element.12.gate_up, bf16[4,2,64,256]{3,2,1,0:T(8,128)(2,1)S(1)} %get-tuple-element.13.x_last, ...), custom_call_target="tpu_custom_call" | custom-call | tf_op jit(solution)/shard_map/pallas_call | solution.py:133
  91.9 5.6 %collective-permute-start.8 = (bf16[3,64,2048]{2,1,0:T(8,128)(2,1)S(1)}, bf16[3,64,2048]{2,1,0:T(8,128)(2,1)S(1)}, u32[]{:S(2)}, u32[]{:S(2)}) collective-permute-start(bf16[3,64,2048]{2,1,0:T(8,128)(2,1)S(1)} %get-tuple-element.18), channel_id=1, source_target_pairs={{0,1},{1,0},{2,3},{3,2},{4,5},{5,4},{6,7},{7,6},{8,9},{9,8},{10,11... | collective-permute-start | bytes 2359304 | tf_op jit(solution)/shard_map/ppermute | solution.py:163
  97.5 1.9 %collective-permute-start.7 = (bf16[64,2048]{1,0:T(8,128)(2,1)S(1)}, bf16[64,2048]{1,0:T(8,128)(2,1)S(1)}, u32[]{:S(2)}, u32[]{:S(2)}) collective-permute-start(bf16[64,2048]{1,0:T(8,128)(2,1)S(1)} %get-tuple-element.16), channel_id=1, source_target_pairs={{0,1},{1,0},{2,3},{3,2},{4,5},{5,4},{6,7},{7,6},{8,9},{9,8},{10,11... | collective-permute-start | bytes 786440 | tf_op jit(solution)/shard_map/ppermute | solution.py:164
  99.5 1.7 %shard_map.64 = (bf16[3,64,2048]{2,1,0:T(8,128)(2,1)S(1)}, bf16[64,2048]{1,0:T(8,128)(2,1)S(1)}) custom-call(s32[4]{0:T(128)S(1)} %get-tuple-element.22.ids, f32[2,4,2,64,384]{4,3,2,1,0:T(8,128)S(1)} %get-tuple-element.12.gate_up, bf16[4,2,64,256]{3,2,1,0:T(8,128)(2,1)S(1)} %get-tuple-element.13.x_last, ...), custom_call_target="tpu_custom_call" | custom-call | tf_op jit(solution)/shard_map/pallas_call | solution.py:133
  101.2 0.0 copy-start.2
  101.2 0.0 collective-permute-done.8
  101.2 0.3 fusion.3
  101.5 3.6 %collective-permute-start.10 = (bf16[64,2048]{1,0:T(8,128)(2,1)S(1)}, bf16[64,2048]{1,0:T(8,128)(2,1)S(1)}, u32[]{:S(2)}, u32[]{:S(2)}) collective-permute-start(bf16[64,2048]{1,0:T(8,128)(2,1)S(1)} %get-tuple-element.21), channel_id=1, source_target_pairs={{0,2},{2,0},{4,6},{6,4},{1,3},{3,1},{5,7},{7,5},{8,10},{10,8},{12,... | collective-permute-start | bytes 786440 | tf_op jit(solution)/shard_map/ppermute | solution.py:170
  105.2 3.7 %collective-permute-start.11 = (bf16[64,2048]{1,0:T(8,128)(2,1)S(1)}, bf16[64,2048]{1,0:T(8,128)(2,1)S(1)}, u32[]{:S(2)}, u32[]{:S(2)}) collective-permute-start(bf16[64,2048]{1,0:T(8,128)(2,1)S(1)} %get-tuple-element.20), channel_id=1, source_target_pairs={{0,6},{2,4},{4,2},{6,0},{1,7},{3,5},{5,3},{7,1},{8,14},{10,12},{12... | collective-permute-start | bytes 786440 | tf_op jit(solution)/shard_map/ppermute | solution.py:170
  108.9 2.5 %collective-permute-start.9 = (bf16[64,2048]{1,0:T(8,128)(2,1)S(1)}, bf16[64,2048]{1,0:T(8,128)(2,1)S(1)}, u32[]{:S(2)}, u32[]{:S(2)}) collective-permute-start(bf16[64,2048]{1,0:T(8,128)(2,1)S(1)} %get-tuple-element.19), channel_id=1, source_target_pairs={{0,4},{2,6},{4,0},{6,2},{1,5},{3,7},{5,1},{7,3},{8,12},{10,14},{12... | collective-permute-start | bytes 786440 | tf_op jit(solution)/shard_map/ppermute | solution.py:170
  111.4 0.0 collective-permute-done.7
  111.4 0.0 collective-permute-done.10
  111.4 9.5 %collective-permute-done.11 = bf16[64,2048]{1,0:T(8,128)(2,1)S(1)} collective-permute-done((bf16[64,2048]{1,0:T(8,128)(2,1)S(1)}, bf16[64,2048]{1,0:T(8,128)(2,1)S(1)}, u32[]{:S(2)}, u32[]{:S(2)}) %collective-permute-start.11) | collective-permute-done | bytes 262176 | tf_op jit(solution)/shard_map/ppermute | solution.py:170
  121.0 0.0 collective-permute-done.9
  121.0 0.3 multiply_reduce_fusion
  121.3 0.0 copy-done.2
  121.3 0.9 multiply_convert_fusion
  (2 shorter events, 0.0 us)
Async XLA Ops:
  0.0 18.0 %copy-start = (bf16[64,2048]{1,0:T(8,128)(2,1)S(1)}, bf16[64,2048]{1,0:T(8,128)(2,1)}, u32[]{:S(2)}) copy-start(bf16[64,2048]{1,0:T(8,128)(2,1)} %param.6) | copy-start | bytes 786436
  0.0 43.3 %copy-start.1 = (f32[2048]{0:T(1024)S(1)}, f32[2048]{0:T(1024)}, u32[]{:S(2)}) copy-start(f32[2048]{0:T(1024)} %param.7) | copy-start | bytes 24580
  1.7 32.7 %all-to-all-start.1 = ((bf16[8,96,384]{2,1,0:T(8,128)(2,1)}), bf16[8,96,384]{2,1,0:T(8,128)(2,1)S(1)}, u32[]{:S(2)}, u32[]{:S(2)}) async-start(bf16[8,96,384]{2,1,0:T(8,128)(2,1)} %broadcast_in_dim.5), calls=%async_computation.1 | async-start | bytes 1179648 | tf_op jit(solution)/shard_map/all_to_all | solution.py:146
  34.4 17.0 %collective-permute-start.1 = (bf16[8,96,384]{2,1,0:T(8,128)(2,1)S(1)}, bf16[8,96,384]{2,1,0:T(8,128)(2,1)S(1)}, u32[]{:S(2)}, u32[]{:S(2)}) collective-permute-start(bf16[8,96,384]{2,1,0:T(8,128)(2,1)S(1)} %all-to-all-done.1.refs_0_), channel_id=1, source_target_pairs={{0,960},{1,57},{8,968},{9,17},{16,976},{17,9},{24,984},{25,33},{32... | collective-permute-start | bytes 1769480 | tf_op jit(solution)/shard_map/ppermute | solution.py:36
  45.0 36.0 %all-to-all-start = ((bf16[8,64,2048]{2,1,0:T(8,128)(2,1)}), bf16[8,64,2048]{2,1,0:T(8,128)(2,1)}, u32[]{:S(2)}, u32[]{:S(2)}) async-start(bf16[8,64,2048]{2,1,0:T(8,128)(2,1)} %broadcast_in_dim.4), calls=%async_computation | async-start | bytes 4194304 | tf_op jit(solution)/shard_map/all_to_all | solution.py:157
  49.4 11.0 %collective-permute-start = (bf16[8,96,384]{2,1,0:T(8,128)(2,1)S(1)}, bf16[8,96,384]{2,1,0:T(8,128)(2,1)S(1)}, u32[]{:S(2)}, u32[]{:S(2)}) collective-permute-start(bf16[8,96,384]{2,1,0:T(8,128)(2,1)S(1)} %all-to-all-done.1.refs_0_), channel_id=1, source_target_pairs={{0,64},{1,9},{8,72},{9,1},{16,80},{17,25},{24,88},{25,17},{32,96},... | collective-permute-start | bytes 1769480 | tf_op jit(solution)/shard_map/ppermute | solution.py:36
  51.4 15.4 %collective-permute-start.2 = (bf16[8,96,384]{2,1,0:T(8,128)(2,1)S(1)}, bf16[8,96,384]{2,1,0:T(8,128)(2,1)S(1)}, u32[]{:S(2)}, u32[]{:S(2)}) collective-permute-start(bf16[8,96,384]{2,1,0:T(8,128)(2,1)S(1)} %collective-permute-done.1.refs_2_), channel_id=1, source_target_pairs={{0,64},{1,9},{8,72},{9,1},{16,80},{17,25},{24,88},{25,17},{32,96},... | collective-permute-start | bytes 1769480 | tf_op jit(solution)/shard_map/ppermute | solution.py:36
  60.5 12.2 %collective-permute-start.3 = (bf16[8,96,384]{2,1,0:T(8,128)(2,1)S(1)}, bf16[8,96,384]{2,1,0:T(8,128)(2,1)S(1)}, u32[]{:S(2)}, u32[]{:S(2)}) collective-permute-start(bf16[8,96,384]{2,1,0:T(8,128)(2,1)S(1)} %collective-permute-done.refs_1_), channel_id=1, source_target_pairs={{0,960},{1,57},{8,968},{9,17},{16,976},{17,9},{24,984},{25,33},{32... | collective-permute-start | bytes 1769480 | tf_op jit(solution)/shard_map/ppermute | solution.py:36
  66.8 12.2 %collective-permute-start.5 = (bf16[8,96,384]{2,1,0:T(8,128)(2,1)S(1)}, bf16[8,96,384]{2,1,0:T(8,128)(2,1)}, u32[]{:S(2)}, u32[]{:S(2)}) collective-permute-start(bf16[8,96,384]{2,1,0:T(8,128)(2,1)S(1)} %collective-permute-done.2.refs_3_), channel_id=1, source_target_pairs={{0,960},{1,57},{8,968},{9,17},{16,976},{17,9},{24,984},{25,33},{32... | collective-permute-start | bytes 1769480 | tf_op jit(solution)/shard_map/ppermute | solution.py:36
  72.7 11.0 %collective-permute-start.4 = (bf16[8,96,384]{2,1,0:T(8,128)(2,1)S(1)}, bf16[8,96,384]{2,1,0:T(8,128)(2,1)}, u32[]{:S(2)}, u32[]{:S(2)}) collective-permute-start(bf16[8,96,384]{2,1,0:T(8,128)(2,1)S(1)} %collective-permute-done.3.refs_4_), channel_id=1, source_target_pairs={{0,64},{1,9},{8,72},{9,1},{16,80},{17,25},{24,88},{25,17},{32,96},... | collective-permute-start | bytes 1769480 | tf_op jit(solution)/shard_map/ppermute | solution.py:36
  79.0 11.1 %collective-permute-start.6 = (bf16[8,96,384]{2,1,0:T(8,128)(2,1)}, bf16[8,96,384]{2,1,0:T(8,128)(2,1)S(1)}, u32[]{:S(2)}, u32[]{:S(2)}) collective-permute-start(bf16[8,96,384]{2,1,0:T(8,128)(2,1)} %collective-permute-done.5.refs_6_), channel_id=1, source_target_pairs={{0,64},{1,9},{8,72},{9,1},{16,80},{17,25},{24,88},{25,17},{32,96},... | collective-permute-start | bytes 1769480 | tf_op jit(solution)/shard_map/ppermute | solution.py:36
  91.9 9.4 %collective-permute-start.8 = (bf16[3,64,2048]{2,1,0:T(8,128)(2,1)S(1)}, bf16[3,64,2048]{2,1,0:T(8,128)(2,1)S(1)}, u32[]{:S(2)}, u32[]{:S(2)}) collective-permute-start(bf16[3,64,2048]{2,1,0:T(8,128)(2,1)S(1)} %get-tuple-element.18), channel_id=1, source_target_pairs={{0,1},{1,0},{2,3},{3,2},{4,5},{5,4},{6,7},{7,6},{8,9},{9,8},{10,11... | collective-permute-start | bytes 2359304 | tf_op jit(solution)/shard_map/ppermute | solution.py:163
  97.5 13.9 %collective-permute-start.7 = (bf16[64,2048]{1,0:T(8,128)(2,1)S(1)}, bf16[64,2048]{1,0:T(8,128)(2,1)S(1)}, u32[]{:S(2)}, u32[]{:S(2)}) collective-permute-start(bf16[64,2048]{1,0:T(8,128)(2,1)S(1)} %get-tuple-element.16), channel_id=1, source_target_pairs={{0,1},{1,0},{2,3},{3,2},{4,5},{5,4},{6,7},{7,6},{8,9},{9,8},{10,11... | collective-permute-start | bytes 786440 | tf_op jit(solution)/shard_map/ppermute | solution.py:164
  101.2 20.0 %copy-start.2 = (f32[2048]{0:T(1024)S(1)}, f32[2048]{0:T(1024)}, u32[]{:S(2)}) copy-start(f32[2048]{0:T(1024)} %param.11) | copy-start | bytes 24580
  101.5 9.9 %collective-permute-start.10 = (bf16[64,2048]{1,0:T(8,128)(2,1)S(1)}, bf16[64,2048]{1,0:T(8,128)(2,1)S(1)}, u32[]{:S(2)}, u32[]{:S(2)}) collective-permute-start(bf16[64,2048]{1,0:T(8,128)(2,1)S(1)} %get-tuple-element.21), channel_id=1, source_target_pairs={{0,2},{2,0},{4,6},{6,4},{1,3},{3,1},{5,7},{7,5},{8,10},{10,8},{12,... | collective-permute-start | bytes 786440 | tf_op jit(solution)/shard_map/ppermute | solution.py:170
  105.2 15.8 %collective-permute-start.11 = (bf16[64,2048]{1,0:T(8,128)(2,1)S(1)}, bf16[64,2048]{1,0:T(8,128)(2,1)S(1)}, u32[]{:S(2)}, u32[]{:S(2)}) collective-permute-start(bf16[64,2048]{1,0:T(8,128)(2,1)S(1)} %get-tuple-element.20), channel_id=1, source_target_pairs={{0,6},{2,4},{4,2},{6,0},{1,7},{3,5},{5,3},{7,1},{8,14},{10,12},{12... | collective-permute-start | bytes 786440 | tf_op jit(solution)/shard_map/ppermute | solution.py:170
  108.9 12.1 %collective-permute-start.9 = (bf16[64,2048]{1,0:T(8,128)(2,1)S(1)}, bf16[64,2048]{1,0:T(8,128)(2,1)S(1)}, u32[]{:S(2)}, u32[]{:S(2)}) collective-permute-start(bf16[64,2048]{1,0:T(8,128)(2,1)S(1)} %get-tuple-element.19), channel_id=1, source_target_pairs={{0,4},{2,6},{4,0},{6,2},{1,5},{3,7},{5,1},{7,3},{8,12},{10,14},{12... | collective-permute-start | bytes 786440 | tf_op jit(solution)/shard_map/ppermute | solution.py:170
